TPU v7x, 32 devices: a whole 2x2x4 slice. The times are simulated.
32 devices in a mesh: sp: 4 (over y, x), dp: 8 (over z, core).
Axes of the slice: x: 2, y: 2, z: 4, core: 2. Of those that a mesh axis runs over, the one named last changes fastest.
Arguments:
- value_half: bfloat16 [8, 1024, 2048], P('dp', 'sp'), may hold values from -6 to 6
- gate_half: bfloat16 [8, 1024, 2048], P('dp', 'sp'), may hold values from -6 to 6
- upstream: bfloat16 [8, 1024, 2048], P('dp', 'sp'), may hold values from -6 to 6
- conv_taps: float32 [31, 2048], P(None, 'sp'), may hold values from -1 to 1
- norm_gain: float32 [2048], replicated, may hold values from 0.1 to 1.9
- out_weight: bfloat16 [2048, 2048], P('dp'), may hold values from -0.125 to 0.125
Outputs:
- grad_value: bfloat16 [8, 1024, 2048], P('dp', 'sp')
- grad_gate: bfloat16 [8, 1024, 2048], P('dp', 'sp')
- grad_taps: float32 [31, 2048], P(None, 'sp')
- grad_gain: float32 [2048], replicated
- grad_weight: float32 [2048, 2048], P('dp')
All inputs are finite; a program needn't handle non-finite values.
Results may differ from a plain program's by a relative error of at most 0.0062.
Values may be sent and summed in bfloat16 or wider, within the bound.
A program may use at most 128 MiB of HBM per device.

v0:
```python
import functools

import jax
import jax.numpy as jnp
from jax import lax
from jax.experimental import pallas as pl
from jax.experimental.pallas import tpu as pltpu
from jax.sharding import PartitionSpec as P

NORM_EPS = 1e-05
VMEM = pl.BlockSpec(memory_space=pltpu.VMEM)


def when(condition, act):
    if condition is None:
        act()
    else:
        pl.when(condition)(lambda: act())


class Copies:
    def __init__(self, send, recv, local):
        self.send, self.recv, self.local = send, recv, local
        self.n_remote = self.n_local = 0
        self.remote, self.locals = [], []

    def start(self, src, dst, target, sends=None, receives=None):
        i = self.n_remote
        self.n_remote += 1
        copy = pltpu.make_async_remote_copy(
            src_ref=src,
            dst_ref=dst,
            send_sem=self.send.at[i],
            recv_sem=self.recv.at[i],
            device_id=target,
            device_id_type=pl.DeviceIdType.MESH,
        )
        when(sends, copy.start)
        self.remote.append([copy, False, sends, receives])
        return len(self.remote) - 1

    def keep(self, src, dst):
        copy = pltpu.make_async_copy(src, dst, self.local.at[self.n_local])
        self.n_local += 1
        copy.start()
        self.locals.append(copy)

    def arrive(self, i):
        when(self.remote[i][3], self.remote[i][0].wait_recv)
        self.remote[i][1] = True

    def finish(self):
        for copy, arrived, sends, receives in self.remote:
            if not arrived:
                when(receives, copy.wait_recv)
            when(sends, copy.wait_send)
        for copy in self.locals:
            copy.wait()


def greet(axes):
    barrier = pltpu.get_barrier_semaphore()
    count = 0
    for axis in axes:
        n = lax.axis_size(axis)
        me = lax.axis_index(axis)
        for k in range(1, n):
            pl.semaphore_signal(
                barrier,
                inc=1,
                device_id={axis: lax.rem(me + k, n)},
                device_id_type=pl.DeviceIdType.MESH,
            )
            count += 1
    pl.semaphore_wait(barrier, count)


def direct(copies, kind, axis, src, dst):
    n = lax.axis_size(axis)
    me = lax.axis_index(axis)
    if kind == "next" or kind == "prev":
        copies.start(src, dst, {axis: lax.rem(me + (1 if kind == "next" else n - 1), n)})
        return
    if kind == "pair":
        copies.start(src, dst, {axis: me + 1 - 2 * lax.rem(me, 2)})
        return
    if kind == "rows":
        nz, z, c = n // 2, me // 2, lax.rem(me, 2)
        copies.keep(src.at[z], dst.at[z])
        for k in range(1, nz):
            peer = lax.rem(z + k, nz)
            copies.start(src.at[peer], dst.at[z], {axis: 2 * peer + c})
        return
    copies.keep(src.at[me] if kind == "scatter" else src, dst.at[me])
    for k in range(1, n):
        peer = lax.rem(me + k, n)
        copies.start(src.at[peer] if kind == "scatter" else src, dst.at[me], {axis: peer})


def spread_gather(copies, src, dst):
    ns, nz = lax.axis_size("sp"), lax.axis_size("dp") // 2
    s, d = lax.axis_index("sp"), lax.axis_index("dp")
    z, c = d // 2, lax.rem(d, 2)
    partner = {"dp": d + 1 - 2 * c}
    first = [
        copies.start(src.at[s], dst.at[d, s], {"dp": 2 * lax.rem(z + k, nz) + c})
        for k in range(1, nz)
    ]
    yield
    copies.keep(src, dst.at[d])
    copies.start(src, dst.at[d], partner)
    second = {}
    for k in range(1, nz):
        copies.arrive(first[k - 1])
        piece = dst.at[2 * lax.rem(z + nz - k, nz) + c, s]
        for j in range(1, ns):
            second[k, j] = copies.start(piece, piece, {"sp": lax.rem(s + j, ns)})
        copies.start(piece, piece, partner)
    yield
    for k in range(1, nz):
        for j in range(1, ns):
            copies.arrive(second[k, j])
            piece = dst.at[2 * lax.rem(z + nz - k, nz) + c, lax.rem(s + ns - j, ns)]
            copies.start(piece, piece, partner)


def line_gather(copies, src, dst):
    nz = lax.axis_size("dp") // 2
    d = lax.axis_index("dp")
    z, c = d // 2, lax.rem(d, 2)
    partner = {"dp": d + 1 - 2 * c}
    up = {"dp": 2 * lax.rem(z + 1, nz) + c}
    down = {"dp": 2 * lax.rem(z + nz - 1, nz) + c}
    below, above = {}, {}

    def send(k):
        low, high = 2 * lax.rem(z + nz - k, nz) + c, 2 * lax.rem(z + k, nz) + c
        low_src, high_src = (dst.at[low], dst.at[high]) if k else (src, src)
        below[k] = copies.start(
            low_src, dst.at[low], up, jnp.logical_and(z >= k, z < nz - 1), z >= k + 1
        )
        above[k] = copies.start(
            high_src, dst.at[high], down, jnp.logical_and(z + k < nz, z > 0), z + k + 1 < nz
        )

    send(0)
    yield
    copies.keep(src, dst.at[d])
    copies.start(src, dst.at[d], partner)
    for k in range(1, nz):
        copies.arrive(below[k - 1])
        copies.arrive(above[k - 1])
        if k < nz - 1:
            send(k)
        low, high = dst.at[2 * lax.rem(z + nz - k, nz) + c], dst.at[2 * lax.rem(z + k, nz) + c]
        copies.start(low, low, partner, z >= k, z >= k)
        copies.start(high, high, partner, z + k < nz, z + k < nz)
        yield


def run(axes, items, *refs):
    n = len(items)
    copies = Copies(*refs[2 * n :])
    greet(axes)
    waiting = []
    for i, (kind, axis) in enumerate(items):
        src, dst = refs[i], refs[n + i]
        if kind == "spread":
            waiting.append(spread_gather(copies, src, dst))
        elif kind == "line":
            waiting.append(line_gather(copies, src, dst))
        elif kind == "later":
            waiting.append(later(copies, axis, src, dst))
        else:
            direct(copies, kind, axis, src, dst)
    while waiting:
        waiting = [steps for steps in waiting if next(steps, waiting) is None]
    copies.finish()


def later(copies, axis, src, dst):
    yield
    direct(copies, "scatter", axis, src, dst)


def exchange(collective_id, *items):
    ns, nd = lax.axis_size("sp"), lax.axis_size("dp")
    shapes, remote, local = [], 0, 0
    for kind, axis, x in items:
        n = lax.axis_size(axis)
        if kind == "rows":
            shape = x.shape
            remote += n // 2 - 1
            local += 1
        elif kind in ("next", "prev", "pair"):
            shape = x.shape
            remote += 1
        elif kind in ("scatter", "later"):
            shape = x.shape
            remote += n - 1
            local += 1
        else:
            shape = (n,) + x.shape
            local += 1
            if kind == "gather":
                remote += n - 1
            elif kind == "spread":
                remote += (nd // 2 - 1) * 2 * ns + 1
            else:
                remote += (nd // 2 - 1) * 4 + 1
        shapes.append(jax.ShapeDtypeStruct(shape, x.dtype))
    axes = tuple(a for a in ("sp", "dp") if any(axis == a or kind == "spread" for kind, axis, _ in items))
    return pl.pallas_call(
        functools.partial(run, axes, tuple((kind, axis) for kind, axis, _ in items)),
        out_shape=shapes,
        in_specs=[VMEM] * len(items),
        out_specs=[VMEM] * len(items),
        scratch_shapes=[
            pltpu.SemaphoreType.DMA((remote,)),
            pltpu.SemaphoreType.DMA((remote,)),
            pltpu.SemaphoreType.DMA((max(local, 1),)),
        ],
        compiler_params=pltpu.CompilerParams(
            collective_id=collective_id, has_side_effects=True, vmem_limit_bytes=48 * 1024 * 1024
        ),
    )(*[x for _, _, x in items])


def body(value_half, gate_half, upstream, conv_taps, norm_gain, out_weight):
    f32 = jnp.float32
    tap_count = conv_taps.shape[0]
    halo = tap_count - 1
    nsp, ndp = lax.axis_size("sp"), lax.axis_size("dp")
    at_start = lax.axis_index("sp") == 0
    at_end = lax.axis_index("sp") == nsp - 1
    edge = (halo + 15) // 16 * 16

    value = value_half[0].astype(f32)
    gate = gate_half[0].astype(f32)
    length = value.shape[0]
    channels = value.shape[1]
    up = upstream[0]
    rows = out_weight.shape[0]

    tail = (value[length - edge :] * jax.nn.sigmoid(gate[length - edge :])).astype(jnp.bfloat16)
    up_blocks = jnp.swapaxes(up.reshape(length, ndp, rows), 0, 1)
    before, taps = exchange(1, ("next", "sp", tail), ("gather", "sp", conv_taps))
    before = jnp.where(at_start, 0, before)[edge - halo :]
    taps = jnp.swapaxes(taps, 0, 1).reshape(tap_count, channels)
    sig_gate = jax.nn.sigmoid(gate)
    glu = (value * sig_gate).astype(jnp.bfloat16)
    padded = jnp.concatenate([before, glu], axis=0).astype(f32)
    conv = jnp.zeros((length, padded.shape[1]), f32)
    for j in range(tap_count):
        conv = conv + taps[j] * padded[j : j + length]
    conv = conv.astype(jnp.bfloat16).astype(f32)
    mean = jnp.mean(conv, axis=-1, keepdims=True)
    centered = conv - mean
    inv = lax.rsqrt(jnp.mean(centered * centered, axis=-1, keepdims=True) + NORM_EPS)
    normed = centered * inv
    scaled = normed * norm_gain
    sig = jax.nn.sigmoid(scaled)
    activated = (scaled * sig).astype(jnp.bfloat16)

    half = channels // 2
    nz, piece = ndp // 2, rows // nsp
    core = lax.rem(lax.axis_index("dp"), 2)
    by_core = up.reshape(length, nz, 2, nsp, piece)

    def partial(which):
        columns = lax.dynamic_index_in_dim(by_core, which, 2, keepdims=False)
        columns = jnp.swapaxes(columns, 1, 2).reshape(length, nsp * nz * piece)
        return lax.dot_general(
            columns, activated[:, half:], (((0,), (0,)), ((), ())), preferred_element_type=f32
        )

    weight, act_all, up_columns, from_partner = exchange(
        2,
        ("spread", "dp", out_weight.reshape(nsp, rows // nsp, channels)),
        ("line", "dp", activated[:, :half]),
        ("later", "dp", up_blocks),
        ("pair", "dp", partial(1 - core).astype(jnp.bfloat16)),
    )
    weight = weight.reshape(ndp * rows, channels)
    act_all = act_all.reshape(ndp * length, half)
    up_columns = up_columns.reshape(ndp * length, rows)
    owned = lax.dot_general(
        up_columns, act_all, (((0,), (0,)), ((), ())), preferred_element_type=f32
    )
    summed = (partial(core) + from_partner.astype(f32)).astype(jnp.bfloat16)
    summed = summed.reshape(nsp, nz, piece, half)

    grad_act = jnp.dot(up, weight, preferred_element_type=f32)
    grad_scaled = grad_act * sig * (1.0 + scaled * (1.0 - sig))
    gain_part = jnp.sum(grad_scaled * normed, axis=0)
    g = grad_scaled * norm_gain
    grad_conv = inv * (
        g
        - jnp.mean(g, axis=-1, keepdims=True)
        - normed * jnp.mean(g * normed, axis=-1, keepdims=True)
    )
    grad_conv = grad_conv.astype(jnp.bfloat16)
    after, gain_got, owned_got, summed_got = exchange(
        3,
        ("prev", "sp", grad_conv[:edge]),
        ("gather", "sp", gain_part[None]),
        ("scatter", "sp", owned.astype(jnp.bfloat16).reshape(nsp, piece, half)),
        ("scatter", "sp", summed),
    )
    after = jnp.where(at_end, 0, after)[:halo]
    extended = jnp.concatenate([grad_conv, after], axis=0).astype(f32)
    here = grad_conv.astype(f32)
    grad_glu = jnp.zeros_like(here)
    terms = []
    for j in range(tap_count):
        first = halo - j
        grad_glu = grad_glu + taps[j] * extended[first : first + length]
        terms.append(jnp.sum(here * padded[j : j + length], axis=0))
    grad_glu = grad_glu.astype(jnp.bfloat16).astype(f32)
    grad_value = (grad_glu * sig_gate).astype(jnp.bfloat16)
    grad_gate = (grad_glu * value * sig_gate * (1.0 - sig_gate)).astype(jnp.bfloat16)

    width = conv_taps.shape[1]
    tap_blocks = jnp.swapaxes(jnp.stack(terms).reshape(tap_count, nsp, width), 0, 1)
    gain_got, tap_got, low_weight, high_got = exchange(
        4,
        ("gather", "dp", jnp.sum(gain_got, axis=0)),
        ("scatter", "sp", tap_blocks),
        ("gather", "sp", jnp.sum(owned_got.astype(f32), axis=0).astype(jnp.bfloat16)),
        ("rows", "dp", jnp.sum(summed_got.astype(f32), axis=0).astype(jnp.bfloat16)),
    )
    tap_got, high_weight = exchange(
        5,
        ("gather", "dp", jnp.sum(tap_got, axis=0)),
        ("gather", "sp", jnp.sum(high_got.astype(f32), axis=0).astype(jnp.bfloat16)),
    )
    grad_gain = jnp.sum(gain_got, axis=0)[0]
    grad_taps = jnp.sum(tap_got, axis=0)
    grad_weight = jnp.concatenate(
        [low_weight.reshape(rows, half), high_weight.reshape(rows, half)], axis=1
    ).astype(f32)
    return (grad_value[None], grad_gate[None], grad_taps, grad_gain, grad_weight)


def solution(mesh):
    tokens = P("dp", "sp", None)
    return jax.shard_map(
        body,
        mesh=mesh,
        in_specs=(tokens, tokens, tokens, P(None, "sp"), P(), P("dp", None)),
        out_specs=(tokens, tokens, P(None, "sp"), P(), P("dp", None)),
        check_vma=False,
    )
```

profile of v0, /device:TPU:1, one launch (start us, length us, event | category | flops | bytes accessed | tf_op | source)
XLA Modules:
  0.0 236.0 jit_solution(403880889660721539)
XLA Ops:
  0.6 1.5 copy.16
  2.3 0.8 copy-done.10
  3.1 0.8 copy.21
  3.9 0.8 copy.19
  4.8 1.5 copy.17
  6.3 0.6 fusion.88
  7.4 0.5 copy-done.1
  7.9 10.1 %shard_map.101 = (bf16[32,2048]{1,0:T(8,128)(2,1)S(1)}, f32[4,31,512]{2,1,0:T(8,128)S(1)}) custom-call(bf16[32,2048]{1,0:T(8,128)(2,1)S(1)} %fusion.100.refs_0_, f32[31,512]{1,0:T(8,128)S(1)} %copy-done.1), custom_call_target="tpu_custom_call" | custom-call | tf_op jit(solution)/shard_map/pallas_call | solution.py:213
  18.7 11.0 %convert_reduce_fusion = (f32[256]{0:T(256)S(1)}, bf16[256,2048]{1,0:T(8,128)(2,1)S(1)}) fusion(f32[286,2048]{1,0:T(8,128)S(1)} %maximum_convert_fusion, f32[2048]{0:T(1024)S(1)} %bitcast.170, f32[2048]{0:T(1024)S(1)} %bitcast.172, f32[2048]{0:T(1024)S(1)} %bitcast.174, f32[2048]{0:T(1024)S(1)} %bitcast.176, f32[2048]{0:T(1024)S(1)} %bitcast.178, ...), kind=kLoop, calls=%fused_computation.38 | loop fusion | flops 33554176 | bytes 66315264 | tf_op jit(solution)/shard_map/reduce_sum | solution.py:257
  29.8 0.4 fusion.21
  30.3 0.9 fusion.14
  31.2 1.0 copy-done.11
  32.2 2.0 convolution_convert_fusion.refs_3_
  34.3 93.9 %shard_map.102 = (bf16[8,4,64,2048]{3,2,1,0:T(8,128)(2,1)}, bf16[8,256,1024]{2,1,0:T(8,128)(2,1)}, bf16[8,256,256]{2,1,0:T(8,128)(2,1)S(1)}, bf16[1024,1024]{1,0:T(8,128)(2,1)S(1)}) custom-call(bf16[4,64,2048]{2,1,0:T(8,128)(2,1)S(1)} %bitcast.132, bf16[256,1024]{1,0:T(8,128)(2,1)S(1)} %slice.564.refs_1_, bf16[8,256,256]{2,1,0:T(8,128)(2,1)S(1)} %bitcast.130, ...), custom_call_target="tpu_custom_call" | custom-call | tf_op jit(solution)/shard_map/pallas_call | solution.py:213
  128.2 6.2 %fusion.20 = (f32[2048]{0:T(1024)S(1)}, f32[256]{0:T(256)S(1)}, f32[256]{0:T(256)S(1)}, f32[256,2048]{1,0:T(8,128)S(1)}) fusion(bf16[256,2048]{1,0:T(8,128)(2,1)S(1)} %get-tuple-element.75, f32[256]{0:T(256)S(1)} %add_rsqrt_fusion, f32[256]{0:T(256)S(1)} %broadcast_multiply_fusion.2, f32[2048]{0:T(1024)S(1)} %copy-done.44, ...), kind=kOutput, calls=%fused_computation.57 | convolution fusion | flops 2156918272 | bytes 12603392 | tf_op jit(solution)/shard_map/dot_general | solution.py:293
  134.4 7.2 %fusion.56 = (f32[2048]{0:T(1024)}, f32[2048]{0:T(1024)}, f32[2048]{0:T(1024)}, f32[2048]{0:T(1024)}, f32[2048]{0:T(1024)}, /*index=5*/f32[2048]{0:T(1024)}, f32...) fusion(f32[286,2048]{1,0:T(8,128)S(1)} %maximum_convert_fusion,, ...), kind=kLoop, calls=%fused_computation.93 | loop fusion | flops 24080384 | bytes 42102784 | tf_op jit(solution)/shard_map/reduce_sum | solution.py:318
  141.6 4.4 %fusion.55 = (f32[2048]{0:T(1024)}, f32[2048]{0:T(1024)}, f32[2048]{0:T(1024)}, f32[2048]{0:T(1024)}, f32[2048]{0:T(1024)}, /*index=5*/f32[2048]{0:T(1024)}, f32...) fusion(bf16[256,2048]{1,0:T(8,128)(2,1)S(1)} %get-tuple-element, ...), kind=kLoop, calls=%fused_computation.92 | loop fusion | flops 14129152 | bytes 28418048 | tf_op jit(solution)/shard_map/reduce_sum | solution.py:318
  146.0 3.6 %stack.127 = f32[31,4,512]{2,0,1:T(8,128)S(1)} concatenate(f32[1,4,512]{2,0,1:T(1,128)} %bitcast.218, f32[1,4,512]{2,0,1:T(1,128)} %bitcast.220, f32[1,4,512]{2,0,1:T(1,128)} %bitcast.221, f32[1,4,512]{2,0,1:T(1,128)} %bitcast.222, f32[1,4,512]{2,0,1:T(1,128)} %bitcast.223, f32[1,4,512]{2,0,1:T(1,128)} %bitcast.224, f32[1,4,512]{2,0,1:T(1,128)} %bitcast.225, ...), dimensions={0} | concatenate | bytes 507904 | tf_op jit(solution)/shard_map/stack | solution.py:324
  149.6 0.9 slice.566.refs_0_
  150.6 3.6 %fusion.89 = bf16[256,1024]{1,0:T(8,128)(2,1)S(1)} fusion(bf16[8,256,256]{2,1,0:T(8,128)(2,1)S(1)} %copy-done.3, bf16[8,256,1024]{2,1,0:T(8,128)(2,1)} %get-tuple-element.25), kind=kOutput, calls=%fused_computation.164 | convolution fusion | flops 1074003968 | bytes 5767168 | tf_op jit(solution)/shard_map/dot_general | solution.py:287
  154.2 0.7 add_convert_fusion
  154.9 34.9 %shard_map.103 = (bf16[32,2048]{1,0:T(8,128)(2,1)S(1)}, f32[4,1,2048]{2,1,0:T(1,128)S(1)}, bf16[4,64,1024]{2,1,0:T(8,128)(2,1)S(1)}, bf16[4,4,64,1024]{3,2,1,0:T(8,128)(2,1)S(1)}) custom-call(bf16[32,2048]{1,0:T(8,128)(2,1)S(1)} %slice.566.refs_0_, f32[1,2048]{1,0:T(1,128)S(1)} %bitcast.139, bf16[4,64,1024]{2,1,0:T(8,128)(2,1)S(1)} %bitcast.134, ...), custom_call_target="tpu_custom_call" | custom-call | tf_op jit(solution)/shard_map/pallas_call | solution.py:213
  190.0 0.4 reduce_sum.437.refs_3_
  190.5 14.5 %shard_map.104 = (f32[8,1,2048]{2,1,0:T(1,128)S(1)}, f32[4,31,512]{2,1,0:T(8,128)S(1)}, bf16[4,64,1024]{2,1,0:T(8,128)(2,1)S(1)}, bf16[4,64,1024]{2,1,0:T(8,128)(2,1)S(1)}) custom-call(f32[1,2048]{1,0:T(1,128)S(1)} %bitcast.138, f32[4,31,512]{2,1,0:T(8,128)S(1)} %bitcast.131, bf16[64,1024]{1,0:T(8,128)(2,1)S(1)} %reduce_sum.436.refs_2_, ...), custom_call_target="tpu_custom_call" | custom-call | tf_op jit(solution)/shard_map/pallas_call | solution.py:213
  205.0 0.7 reduce_sum.441
  205.7 15.3 %shard_map.105 = (f32[8,31,512]{2,1,0:T(8,128)S(1)}, bf16[4,64,1024]{2,1,0:T(8,128)(2,1)S(1)}) custom-call(f32[31,512]{1,0:T(8,128)S(1)} %reduce_sum.438.refs_0_, bf16[64,1024]{1,0:T(8,128)(2,1)S(1)} %reduce_sum.439.refs_1_), custom_call_target="tpu_custom_call" | custom-call | tf_op jit(solution)/shard_map/pallas_call | solution.py:213
  221.1 0.7 reduce_sum.440
  221.8 1.6 maximum_convert_fusion.2
  223.7 0.8 copy-done.5
  224.5 0.3 copy-done.9
  225.0 9.5 %fusion.90 = (bf16[1,256,2048]{2,1,0:T(8,128)(2,1)}, bf16[256,2048]{1,0:T(8,128)(2,1)S(1)}) fusion(bf16[1,256,2048]{2,1,0:T(8,128)(2,1)S(1)} %copy-done.9, bf16[1,256,2048]{2,1,0:T(8,128)(2,1)S(1)} %copy-done.5, f32[286,2048]{1,0:T(8,128)S(1)} %maximum_convert_fusion.1, f32[2048]{0:T(1024)S(1)} %bitcast.171, f32[2048]{0:T(1024)S(1)} %bitcast.173, ...), kind=kLoop, calls=%fused_computation.167 | loop fusion | flops 38273024 | bytes 69459968 | tf_op jit(solution)/shard_map/broadcast_in_dim | solution.py:342
  234.5 1.6 fusion.91
  (103 shorter events, 1.9 us)
Async XLA Ops:
  3.1 3.1 %copy-start.4 = (bf16[1,256,2048]{2,1,0:T(8,128)(2,1)S(1)}, bf16[1,256,2048]{2,1,0:T(8,128)(2,1)}, u32[]{:S(2)}) copy-start(bf16[1,256,2048]{2,1,0:T(8,128)(2,1)} %param.7) | copy-start | bytes 3145732
  3.1 3.1 %copy-start.8 = (bf16[1,256,2048]{2,1,0:T(8,128)(2,1)S(1)}, bf16[1,256,2048]{2,1,0:T(8,128)(2,1)}, u32[]{:S(2)}) copy-start(bf16[1,256,2048]{2,1,0:T(8,128)(2,1)} %param.6) | copy-start | bytes 3145732
  18.2 11.5 %copy-start.16 = (f32[1,4,512]{2,0,1:T(1,128)}, f32[1,4,512]{2,0,1:T(1,128)S(1)}, u32[]{:S(2)}) copy-start(f32[1,4,512]{2,0,1:T(1,128)S(1)} %get-tuple-element.83) | copy-start | bytes 24580
  18.2 11.5 %copy-start.18 = (f32[1,4,512]{2,0,1:T(1,128)}, f32[1,4,512]{2,0,1:T(1,128)S(1)}, u32[]{:S(2)}) copy-start(f32[1,4,512]{2,0,1:T(1,128)S(1)} %get-tuple-element.84) | copy-start | bytes 24580
  18.2 11.5 %copy-start.20 = (f32[1,4,512]{2,0,1:T(1,128)}, f32[1,4,512]{2,0,1:T(1,128)S(1)}, u32[]{:S(2)}) copy-start(f32[1,4,512]{2,0,1:T(1,128)S(1)} %get-tuple-element.85) | copy-start | bytes 24580
  18.2 11.5 %copy-start.22 = (f32[1,4,512]{2,0,1:T(1,128)}, f32[1,4,512]{2,0,1:T(1,128)S(1)}, u32[]{:S(2)}) copy-start(f32[1,4,512]{2,0,1:T(1,128)S(1)} %get-tuple-element.86) | copy-start | bytes 24580
  18.2 11.5 %copy-start.24 = (f32[1,4,512]{2,0,1:T(1,128)}, f32[1,4,512]{2,0,1:T(1,128)S(1)}, u32[]{:S(2)}) copy-start(f32[1,4,512]{2,0,1:T(1,128)S(1)} %get-tuple-element.87) | copy-start | bytes 24580
  18.2 11.5 %copy-start.26 = (f32[1,4,512]{2,0,1:T(1,128)}, f32[1,4,512]{2,0,1:T(1,128)S(1)}, u32[]{:S(2)}) copy-start(f32[1,4,512]{2,0,1:T(1,128)S(1)} %get-tuple-element.88) | copy-start | bytes 24580
  18.3 11.5 %copy-start.28 = (f32[1,4,512]{2,0,1:T(1,128)}, f32[1,4,512]{2,0,1:T(1,128)S(1)}, u32[]{:S(2)}) copy-start(f32[1,4,512]{2,0,1:T(1,128)S(1)} %get-tuple-element.89) | copy-start | bytes 24580
  18.3 11.5 %copy-start.30 = (f32[1,4,512]{2,0,1:T(1,128)}, f32[1,4,512]{2,0,1:T(1,128)S(1)}, u32[]{:S(2)}) copy-start(f32[1,4,512]{2,0,1:T(1,128)S(1)} %get-tuple-element.90) | copy-start | bytes 24580
  18.3 11.5 %copy-start.32 = (f32[1,4,512]{2,0,1:T(1,128)}, f32[1,4,512]{2,0,1:T(1,128)S(1)}, u32[]{:S(2)}) copy-start(f32[1,4,512]{2,0,1:T(1,128)S(1)} %get-tuple-element.91) | copy-start | bytes 24580
  18.3 11.5 %copy-start.34 = (f32[1,4,512]{2,0,1:T(1,128)}, f32[1,4,512]{2,0,1:T(1,128)S(1)}, u32[]{:S(2)}) copy-start(f32[1,4,512]{2,0,1:T(1,128)S(1)} %get-tuple-element.92) | copy-start | bytes 24580
  18.3 11.5 %copy-start.36 = (f32[1,4,512]{2,0,1:T(1,128)}, f32[1,4,512]{2,0,1:T(1,128)S(1)}, u32[]{:S(2)}) copy-start(f32[1,4,512]{2,0,1:T(1,128)S(1)} %get-tuple-element.93) | copy-start | bytes 24580
  18.3 11.5 %copy-start.38 = (f32[1,4,512]{2,0,1:T(1,128)}, f32[1,4,512]{2,0,1:T(1,128)S(1)}, u32[]{:S(2)}) copy-start(f32[1,4,512]{2,0,1:T(1,128)S(1)} %get-tuple-element.94) | copy-start | bytes 24580
  18.3 11.5 %copy-start.40 = (f32[1,4,512]{2,0,1:T(1,128)}, f32[1,4,512]{2,0,1:T(1,128)S(1)}, u32[]{:S(2)}) copy-start(f32[1,4,512]{2,0,1:T(1,128)S(1)} %get-tuple-element.95) | copy-start | bytes 24580
  18.3 11.5 %copy-start.42 = (f32[1,4,512]{2,0,1:T(1,128)}, f32[1,4,512]{2,0,1:T(1,128)S(1)}, u32[]{:S(2)}) copy-start(f32[1,4,512]{2,0,1:T(1,128)S(1)} %get-tuple-element.96) | copy-start | bytes 24580
  18.7 11.6 %copy-start.44 = (f32[2048]{0:T(1024)S(1)}, f32[2048]{0:T(1024)}, u32[]{:S(2)}) copy-start(f32[2048]{0:T(1024)} %param.10) | copy-start | bytes 24580
  29.8 2.4 %copy-start.14 = (bf16[256,4,4,64]{0,3,2,1:T(8,128)(2,1)S(1)}, bf16[256,4,4,64]{0,3,2,1:T(8,128)(2,1)}, u32[]{:S(2)}) copy-start(bf16[256,4,4,64]{0,3,2,1:T(8,128)(2,1)} %copy.19) | copy-start | bytes 1572868
  31.2 3.1 %copy-start = (bf16[256,2048]{1,0:T(8,128)(2,1)S(1)}, bf16[256,2048]{1,0:T(8,128)(2,1)}, u32[]{:S(2)}) copy-start(bf16[256,2048]{1,0:T(8,128)(2,1)} %param.11) | copy-start | bytes 3145732
  34.3 93.9 %copy-start.15 = (bf16[1,256,2048]{2,1,0:T(8,128)(2,1)S(1)}, bf16[1,256,2048]{2,1,0:T(8,128)(2,1)}, u32[]{:S(2)}) copy-start(bf16[1,256,2048]{2,1,0:T(8,128)(2,1)} %param.8) | copy-start | bytes 3145732
  128.2 6.2 %copy-start.2 = (bf16[8,256,256]{2,1,0:T(8,128)(2,1)}, bf16[8,256,256]{2,1,0:T(8,128)(2,1)S(1)}, u32[]{:S(2)}) copy-start(bf16[8,256,256]{2,1,0:T(8,128)(2,1)S(1)} %get-tuple-element.24) | copy-start | bytes 3145732
  141.6 4.4 %copy-start.6 = (bf16[256,2048]{1,0:T(8,128)(2,1)}, bf16[256,2048]{1,0:T(8,128)(2,1)S(1)}, u32[]{:S(2)}) copy-start(bf16[256,2048]{1,0:T(8,128)(2,1)S(1)} %get-tuple-element.71) | copy-start | bytes 3145732
  141.6 8.9 %copy-start.3 = (bf16[8,256,256]{2,1,0:T(8,128)(2,1)S(1)}, bf16[8,256,256]{2,1,0:T(8,128)(2,1)}, u32[]{:S(2)}) copy-start(bf16[8,256,256]{2,1,0:T(8,128)(2,1)} %copy-done.2) | copy-start | bytes 3145732
  150.6 3.6 %copy-start.12 = (bf16[256,2048]{1,0:T(8,128)(2,1)S(1)}, bf16[256,2048]{1,0:T(8,128)(2,1)}, u32[]{:S(2)}) copy-start(bf16[256,2048]{1,0:T(8,128)(2,1)} %copy-done.11) | copy-start | bytes 3145732
  150.6 3.6 %copy-start.13 = (bf16[256,4,4,64]{0,3,2,1:T(8,128)(2,1)S(1)}, bf16[256,4,4,64]{0,3,2,1:T(8,128)(2,1)}, u32[]{:S(2)}) copy-start(bf16[256,4,4,64]{0,3,2,1:T(8,128)(2,1)} %copy.21) | copy-start | bytes 1572868
  205.7 17.6 %copy-start.7 = (bf16[256,2048]{1,0:T(8,128)(2,1)S(1)}, bf16[256,2048]{1,0:T(8,128)(2,1)}, u32[]{:S(2)}) copy-start(bf16[256,2048]{1,0:T(8,128)(2,1)} %copy-done.6) | copy-start | bytes 3145732
  223.3 1.5 copy-start.9
  223.3 1.5 copy-start.17
  223.3 1.5 copy-start.19
  223.3 1.5 copy-start.21
  223.3 1.5 copy-start.23
  223.4 1.5 copy-start.25
  (13 other events, 17.8 us)
where the time goes:
time: 237 us; the launch traced here: 236 us
  Pallas kernels  169 us (71%)
  other arithmetic  40.2 us (17%)
  local copies, waits for them, and re-layouts  13.1 us (6%)
  matrix products  12.5 us (5%)
    pallas_call x5, Pallas kernels, exchange(): pl.pallas_call(functools.partial(run, axes, tuple(((kind, axis) for kind,...  169 us
    reduce_sum x2, other arithmetic, body(): terms.append(jnp.sum(here * padded[j:j + length], axis=0))  11.6 us
    reduce_sum x1, other arithmetic, body(): mean = jnp.mean(conv, axis=-1, keepdims=True)  11 us
    broadcast_in_dim x1, other arithmetic, body(): grad_gate[None]  9.5 us
    dot_general x1, matrix products, body(): grad_act = jnp.dot(up, weight, preferred_element_type=f32)  6.21 us
    unnamed x91, local copies, waits for them, and re-layouts  5.14 us

commit v1 on v0

--- a/solution.py
+++ b/solution.py
@@ -342,10 +342,587 @@
     return (grad_value[None], grad_gate[None], grad_taps, grad_gain, grad_weight)
 
 
+BLOCK = 64
+LANES = 128
+
+
+class Net:
+    def __init__(self, send, recv, local):
+        self.send, self.recv, self.local = send, recv, local
+        self.n = self.m = 0
+        self.open = []
+        self.landing = []
+
+    def ids(self, count):
+        self.n += count
+        return self.n - count
+
+    def put(self, src, dst, to, slot=None, sends=None):
+        i = self.ids(1)
+        copy = pltpu.make_async_remote_copy(
+            src_ref=src,
+            dst_ref=dst,
+            send_sem=self.send.at[i],
+            recv_sem=self.recv.at[i if slot is None else slot],
+            device_id=to,
+            device_id_type=pl.DeviceIdType.MESH,
+        )
+        copy.start()
+        self.open.append(copy)
+        return copy
+
+    def arrival(self, ref, slot, to):
+        pltpu.make_async_remote_copy(
+            src_ref=ref,
+            dst_ref=ref,
+            send_sem=self.send.at[0],
+            recv_sem=self.recv.at[slot],
+            device_id=to,
+            device_id_type=pl.DeviceIdType.MESH,
+        ).wait_recv()
+
+    def load(self, src, dst):
+        copy = pltpu.make_async_copy(src, dst, self.local.at[self.m])
+        self.m += 1
+        copy.start()
+        return copy
+
+    def finish(self):
+        for copy in self.open:
+            copy.wait_send()
+
+
+def nearest(z, nz, i):
+    low, high = z, nz - 1 - z
+    both = 2 * jnp.minimum(low, high)
+    away = jnp.where(i < both, i // 2 + 1, i - both // 2 + 1)
+    up = jnp.where(i < both, i % 2 == 0, high > low)
+    return jnp.where(up, z + away, z - away)
+
+
+def fused(
+    value_hbm, gate_hbm, up_hbm, taps_hbm, gain_hbm, weight_hbm,
+    grad_value, grad_gate, grad_taps, grad_gain, grad_weight,
+    value, gate, ups, taps, gain, weight, tail, before, padded, conv, scale, acts, act,
+    parts, got_x, got_y, got_xy, got_yx, plane, got_z, final, halves, give_x, give_y,
+    grad_act, head, after, grads, tap_sums, gain_sum, terms, got_terms, got_dp, row_part, both_parts,
+    tap_other, gain_rows,
+    send, recv, local,
+):
+    f32, bf16 = jnp.float32, jnp.bfloat16
+    nsp, ndp = lax.axis_size("sp"), lax.axis_size("dp")
+    nz = ndp // 2
+    s, d = lax.axis_index("sp"), lax.axis_index("dp")
+    z, c = d // 2, lax.rem(d, 2)
+    xn, yn = s + 1 - 2 * lax.rem(s, 2), lax.rem(s + 2, nsp)
+    dg = nsp - 1 - s
+    length, channels = value.shape
+    halo = before.shape[0]
+    tap_count = taps.shape[1]
+    width = taps.shape[2]
+    rows = weight.shape[0] // ndp
+    half = channels // 2
+    side = half // 2
+    quarter = channels // nsp
+    share = 2 * rows // nsp
+    tiles = channels // LANES
+    at_row = tap_count - (terms.shape[1] - 8)
+    net = Net(send, recv, local)
+    to_x, to_y, to_d, partner = {"sp": xn}, {"sp": yn}, {"sp": dg}, {"dp": d + 1 - 2 * c}
+
+    def at_chip(peer):
+        return {"dp": 2 * peer + c}
+
+    def al(i, n):
+        return pl.multiple_of(i, n)
+
+    in_up = net.load(up_hbm.at[0], ups.at[pl.ds(0, length)])
+    in_weight = net.load(weight_hbm, weight.at[pl.ds(al(d * rows, rows), rows)])
+    in_value = net.load(value_hbm.at[0], value)
+    in_gate = net.load(gate_hbm.at[0], gate)
+    in_taps = net.load(taps_hbm, taps.at[s])
+    in_gain = net.load(gain_hbm, gain)
+
+    barrier = pltpu.get_barrier_semaphore()
+    peers = [to_x, to_y, to_d, partner] + [at_chip(lax.rem(z + k, nz)) for k in range(1, nz)]
+    for peer in peers:
+        pl.semaphore_signal(barrier, inc=1, device_id=peer, device_id_type=pl.DeviceIdType.MESH)
+    pl.semaphore_wait(barrier, len(peers))
+
+    def piece(owner, q, h):
+        r = rows // 2
+        return weight.at[
+            pl.ds(al(owner * rows + h * r, r), r), pl.ds(al(q * quarter, quarter), quarter)
+        ]
+
+    hops = [(i, h) for i in range(nz - 1) for h in range(2)]
+    in_weight.wait()
+    w_slots = net.ids(2 * nz)
+    for i, h in hops:
+        peer = nearest(z, nz, i)
+        net.put(piece(d, s, h), piece(d, s, h), at_chip(peer), w_slots + 2 * z + h)
+    in_up.wait()
+    own_rows = weight.at[pl.ds(al(d * rows, rows), rows)]
+    own_weight = net.put(own_rows, own_rows, partner)
+    own_up = net.put(ups.at[pl.ds(0, length)], ups.at[pl.ds(length, length)], partner)
+    in_taps.wait()
+    tap_copies = [net.put(taps.at[s], taps.at[s], to) for to in (to_x, to_y, to_d)]
+
+    arrived = {}
+    mates = {}
+
+    def first(i, h):
+        src = nearest(z, nz, i)
+        owner = 2 * src + c
+        net.arrival(piece(owner, s, h), w_slots + 2 * src + h, partner)
+        p = piece(owner, s, h)
+        arrived[i, h] = [net.put(p, p, to_x), net.put(p, p, to_y)]
+        mates.setdefault(i, []).append(net.put(p, p, partner))
+
+    def second(i, h):
+        owner = 2 * nearest(z, nz, i) + c
+        from_x, from_y = arrived[i, h]
+        px, py = piece(owner, xn, h), piece(owner, yn, h)
+        if h == 0:
+            from_x.wait_recv()
+            arrived[i, h] = net.put(px, px, to_y)
+            from_y.wait_recv()
+        else:
+            from_y.wait_recv()
+            arrived[i, h] = net.put(py, py, to_x)
+            from_x.wait_recv()
+        mates[i] += [net.put(px, px, partner), net.put(py, py, partner)]
+
+    def third(i, h):
+        owner = 2 * nearest(z, nz, i) + c
+        arrived[i, h].wait_recv()
+        p = piece(owner, dg, h)
+        mates[i].append(net.put(p, p, partner))
+
+    weight_steps = []
+    for n in range(len(hops) + 2):
+        if n < len(hops):
+            weight_steps.append(functools.partial(first, *hops[n]))
+        if 1 <= n <= len(hops):
+            weight_steps.append(functools.partial(second, *hops[n - 1]))
+        if n >= 2:
+            weight_steps.append(functools.partial(third, *hops[n - 2]))
+
+    def gather_weight(count):
+        for _ in range(min(count, len(weight_steps))):
+            weight_steps.pop(0)()
+
+    in_value.wait()
+    in_gate.wait()
+    v = value[length - halo :, :].astype(f32)
+    tail[...] = (v * jax.nn.sigmoid(gate[length - halo :, :].astype(f32))).astype(bf16)
+
+    def glu_rows(i, _):
+        r = al(i * 16, 16)
+        v = value[pl.ds(r, 16), :].astype(f32)
+        g = (v * jax.nn.sigmoid(gate[pl.ds(r, 16), :].astype(f32))).astype(bf16)
+        padded[pl.ds(al(r + halo, 8), 16), :] = g.astype(f32)
+        return 0
+
+    lax.fori_loop(0, 2, glu_rows, 0)
+    left = net.put(tail, before, {"sp": lax.rem(s + 1, nsp)})
+    lax.fori_loop(2, length // 16, glu_rows, 0)
+    gather_weight(1)
+    for copy in tap_copies:
+        copy.wait_recv()
+    left.wait_recv()
+    b = before[...].astype(f32)
+    padded[pl.ds(0, halo), :] = jnp.where(s == 0, jnp.zeros_like(b), b)
+
+    per_block = width // LANES
+
+    def tap(t, j):
+        q, lane = t // per_block, lax.rem(t, per_block)
+        return taps[q, pl.ds(j, 1), pl.ds(al(lane * LANES, LANES), LANES)]
+
+    def turned(window, r):
+        return window if r == 0 else pltpu.roll(window, window.shape[0] - r, 0)
+
+    def conv_tile(t, _):
+        cols = pl.ds(al(t * LANES, LANES), LANES)
+
+        def block(i, _):
+            r0 = al(i * BLOCK, BLOCK)
+            window = padded[pl.ds(r0, BLOCK + halo), cols]
+            total = jnp.zeros((BLOCK, LANES), f32)
+            for r in range(8):
+                moved = turned(window, r)
+                for o in range(r, halo + 1, 8):
+                    j = o - (halo - tap_count + 1)
+                    if 0 <= j < tap_count:
+                        total = total + tap(t, j) * moved[o - r : o - r + BLOCK]
+            conv[pl.ds(r0, BLOCK), cols] = total.astype(bf16).astype(f32)
+            return 0
+
+        return lax.fori_loop(0, length // BLOCK, block, 0)
+
+    part = tiles // 4
+    for n in range(4):
+        lax.fori_loop(n * part, (n + 1) * part, conv_tile, 0)
+        gather_weight(1)
+
+    in_gain.wait()
+
+    def norm_rows(i, _):
+        r = al(i * 16, 16)
+        rr = pl.ds(r, 16)
+        x = conv[rr, :]
+        mean = jnp.mean(x, axis=-1, keepdims=True)
+        x = x - mean
+        inv = lax.rsqrt(jnp.mean(x * x, axis=-1, keepdims=True) + NORM_EPS)
+        normed = x * inv
+        conv[rr, :] = normed
+        scale[rr, :] = jnp.broadcast_to(inv, (16, LANES))
+        scaled = normed * gain[...]
+        act[rr, :] = (scaled * jax.nn.sigmoid(scaled)).astype(bf16)
+        return 0
+
+    blocks = length // 16
+    lax.fori_loop(0, blocks // 2, norm_rows, 0)
+    gather_weight(1)
+    lax.fori_loop(blocks // 2, blocks, norm_rows, 0)
+
+    mine = pl.ds(al(c * half, half), half)
+    other = pl.ds(al((1 - c) * half, half), half)
+    act_copy = net.put(act.at[:, other], acts.at[pl.ds(length, length)], partner)
+    acts[pl.ds(0, length), :] = act[:, mine]
+    gather_weight(2)
+    own_up.wait_recv()
+    act_copy.wait_recv()
+
+    def target(k):
+        return nearest(z, nz, nz - 2 - k) if k < nz - 1 else z
+
+    phase_one, phase_two = {}, {}
+
+    def unit(ref, q, h):
+        return ref.at[pl.ds(al(q * share, share), share), pl.ds(h * side, side)]
+
+    def multiply(k):
+        t = target(k)
+        step = min(256, 2 * rows)
+
+        def some(m, _):
+            u = ups[:, pl.ds(al(t * 2 * rows + m * step, step), step)]
+            p = lax.dot_general(u, acts[...], (((0,), (0,)), ((), ())), preferred_element_type=f32)
+            parts[k, pl.ds(al(m * step, step), step), :] = p.astype(bf16)
+            return 0
+
+        lax.fori_loop(0, 2 * rows // step, some, 0)
+
+    def scatter_one(k):
+        p = parts.at[k]
+        phase_one[k] = [
+            net.put(unit(p, dg, 0), got_x.at[k, 1], to_x),
+            net.put(unit(p, dg, 1), got_y.at[k, 1], to_y),
+            net.put(unit(p, xn, 0), got_x.at[k, 0], to_x),
+            net.put(unit(p, yn, 1), got_y.at[k, 0], to_y),
+        ]
+
+    def own(k, q, h):
+        return parts[k, pl.ds(al(q * share, share), share), pl.ds(h * side, side)].astype(f32)
+
+    def scatter_two(k):
+        diag_x, diag_y, mine_x, mine_y = phase_one[k]
+        diag_x.wait_recv()
+        give_y[k] = (own(k, yn, 0) + got_x[k, 1].astype(f32)).astype(bf16)
+        diag_y.wait_recv()
+        give_x[k] = (own(k, xn, 1) + got_y[k, 1].astype(f32)).astype(bf16)
+        phase_two[k] = [
+            net.put(give_y.at[k], got_xy.at[k], to_y),
+            net.put(give_x.at[k], got_yx.at[k], to_x),
+        ]
+        mine_x.wait_recv()
+        mine_y.wait_recv()
+
+    z_slots = net.ids(nz)
+
+    def scatter_three(k):
+        for copy in phase_two[k]:
+            copy.wait_recv()
+        low = own(k, s, 0) + got_x[k, 0].astype(f32) + got_xy[k].astype(f32)
+        high = own(k, s, 1) + got_y[k, 0].astype(f32) + got_yx[k].astype(f32)
+        plane[k, :, pl.ds(0, side)] = low.astype(bf16)
+        plane[k, :, pl.ds(side, side)] = high.astype(bf16)
+        if k < nz - 1:
+            net.put(plane.at[k], got_z.at[z], at_chip(target(k)), z_slots + z)
+
+    multiply(0)
+    gather_weight(2)
+    scatter_one(0)
+    multiply(1)
+    gather_weight(2)
+
+    def product(owner, start):
+        w = weight[pl.ds(al(owner * rows, rows), rows), :]
+        u = ups[pl.ds(0, length), pl.ds(al(owner * rows, rows), rows)]
+        p = jnp.dot(u, w, preferred_element_type=f32)
+        grad_act[...] = p if start else grad_act[...] + p
+
+    product(d, True)
+    own_weight.wait_recv()
+
+    def blocks_of(src):
+        def one(i, _):
+            product(2 * src + i, False)
+            return 0
+
+        lax.fori_loop(0, 2, one, 0)
+
+    product(d + 1 - 2 * c, False)
+    gather_weight(2)
+    scatter_one(1)
+    multiply(2)
+    gather_weight(2)
+    for i in range(nz - 1):
+        gather_weight(2 if i < nz - 2 else len(weight_steps))
+        if i == nz - 2:
+            scatter_one(2)
+            multiply(3)
+        for copy in mates[i]:
+            copy.wait_recv()
+        blocks_of(nearest(z, nz, i))
+    for k in range(3, nz):
+        if k > 3:
+            multiply(k)
+        scatter_one(k)
+
+    gain_sum[...] = jnp.zeros_like(gain_sum)
+
+    def back_rows(i, _):
+        r = al(i * 16, 16)
+        rr = pl.ds(r, 16)
+        normed = conv[rr, :]
+        scaled = normed * gain[...]
+        sig = jax.nn.sigmoid(scaled)
+        gs = grad_act[rr, :] * sig * (1.0 + scaled * (1.0 - sig))
+        gn = gs * normed
+        gain_sum[...] += gn[:8] + gn[8:]
+        g = gs * gain[...]
+        m1 = jnp.mean(g, axis=-1, keepdims=True)
+        m2 = jnp.mean(g * normed, axis=-1, keepdims=True)
+        gc = (scale[rr, 0:1] * (g - m1 - normed * m2)).astype(bf16)
+        grads[rr, :] = gc.astype(f32)
+        return 0
+
+    lax.fori_loop(0, halo // 16, back_rows, 0)
+    head[...] = grads[pl.ds(0, halo), :].astype(bf16)
+    scatter_two(0)
+    right = net.put(head, after, {"sp": lax.rem(s + nsp - 1, nsp)})
+    lax.fori_loop(halo // 16, blocks // 2, back_rows, 0)
+    scatter_three(0)
+    lax.fori_loop(blocks // 2, blocks, back_rows, 0)
+    scatter_two(1)
+    right.wait_recv()
+    a = after[...].astype(f32)
+    grads[pl.ds(length, halo), :] = jnp.where(s == nsp - 1, jnp.zeros_like(a), a)
+
+    tap_sums[...] = jnp.zeros_like(tap_sums)
+
+    def back_tile(t, _):
+        cols = pl.ds(al(t * LANES, LANES), LANES)
+
+        def block(i, _):
+            r0 = al(i * BLOCK, BLOCK)
+            rr = pl.ds(r0, BLOCK)
+            window = grads[pl.ds(r0, BLOCK + halo), cols]
+            total = jnp.zeros((BLOCK, LANES), f32)
+            for r in range(8):
+                moved = turned(window, r)
+                for o in range(r, tap_count, 8):
+                    total = total + tap(t, tap_count - 1 - o) * moved[o - r : o - r + BLOCK]
+            gg = total.astype(bf16).astype(f32)
+            sg = jax.nn.sigmoid(gate[rr, cols].astype(f32))
+            grad_value[rr, cols] = (gg * sg).astype(bf16)
+            grad_gate[rr, cols] = (gg * value[rr, cols].astype(f32) * sg * (1.0 - sg)).astype(bf16)
+            gc = window[:BLOCK]
+            window = padded[pl.ds(r0, BLOCK + halo), cols]
+            for r in range(8):
+                moved = turned(window, r)
+                for o in range(r, halo + 1, 8):
+                    j = o - (halo - tap_count + 1)
+                    if 0 <= j < tap_count:
+                        term = (gc * moved[o - r : o - r + BLOCK]).reshape(BLOCK // 8, 8, LANES)
+                        tap_sums[j, :, cols] += jnp.sum(term, axis=0)
+            return 0
+
+        lax.fori_loop(0, length // BLOCK, block, 0)
+        q, lane = t // per_block, lax.rem(t, per_block)
+        lanes = pl.ds(al(lane * LANES, LANES), LANES)
+        terms[q, pl.ds(0, tap_count), lanes] = jnp.sum(tap_sums[:, :, cols], axis=1)
+        return 0
+
+    order = []
+    for k in range(nz):
+        if k >= 1:
+            order.append(functools.partial(scatter_three, k))
+        if k + 2 <= nz - 1:
+            order.append(functools.partial(scatter_two, k + 2))
+    pieces = 8
+    part = tiles // pieces
+    for n in range(pieces):
+        lax.fori_loop(n * part, (n + 1) * part, back_tile, 0)
+        if n >= 2 and order:
+            order.pop(0)()
+    for q in range(nsp):
+        total = jnp.sum(gain_sum[:, pl.ds(q * width, width)], axis=0, keepdims=True)
+        terms[q, pl.ds(tap_count, 1), :] = total
+    scattered = [
+        net.put(terms.at[peer], got_terms.at[s], to)
+        for peer, to in ((dg, to_d), (xn, to_x), (yn, to_y))
+    ]
+    while order:
+        order.pop(0)()
+    got_terms[s] = terms[s]
+    for copy in scattered:
+        copy.wait_recv()
+    total = got_terms[0]
+    for q in range(1, nsp):
+        total = total + got_terms[q]
+    row_part[...] = total
+    got_dp[z] = total
+    tap_slots = net.ids(nz)
+    for i in range(nz - 1):
+        net.put(row_part, got_dp.at[z], at_chip(nearest(z, nz, i)), tap_slots + z)
+
+    for i in range(nz - 1):
+        src = nearest(z, nz, i)
+        net.arrival(got_z.at[src], z_slots + src, partner)
+    total = plane[nz - 1].astype(f32)
+    for i in range(nz - 1):
+        total = total + got_z[nearest(z, nz, i)].astype(f32)
+    final[pl.ds(al(s * share, share), share), :] = total.astype(bf16)
+
+    def done(q, h):
+        return unit(final, q, h)
+
+    sent = {
+        (axis, h): net.put(done(s, h), done(s, h), to_x if axis == "x" else to_y)
+        for axis, h in (("x", 0), ("y", 1), ("y", 0), ("x", 1))
+    }
+    for i in range(nz - 1):
+        src = nearest(z, nz, i)
+        net.arrival(got_dp.at[src], tap_slots + src, partner)
+    total = got_dp[0]
+    for i in range(1, nz):
+        total = total + got_dp[i]
+    both_parts[...] = total
+    tap_pair = net.put(both_parts, tap_other, partner)
+    sent["x", 0].wait_recv()
+    low = net.put(done(xn, 0), done(xn, 0), to_y)
+    sent["y", 1].wait_recv()
+    high = net.put(done(yn, 1), done(yn, 1), to_x)
+    tap_pair.wait_recv()
+    total = both_parts[...] + tap_other[...]
+    grad_taps[...] = total[:tap_count]
+    gain_rows[s] = total[total.shape[0] - 8 :]
+    gains = [net.put(gain_rows.at[s], gain_rows.at[s], to) for to in (to_d, to_x, to_y)]
+    sent["y", 0].wait_recv()
+    sent["x", 1].wait_recv()
+    low.wait_recv()
+    high.wait_recv()
+    mine_rows = pl.ds(al(c * rows, rows), rows)
+    other_rows = pl.ds(al((1 - c) * rows, rows), rows)
+    last = net.put(final.at[other_rows], halves, partner)
+    grad_weight[:, mine] = final[mine_rows, :].astype(f32)
+    for copy in gains:
+        copy.wait_recv()
+    for q in range(nsp):
+        grad_gain[:, pl.ds(q * width, width)] = gain_rows[q][at_row : at_row + 1]
+    last.wait_recv()
+    grad_weight[:, other] = halves[...].astype(f32)
+    net.finish()
+
+
+def fused_body(value_half, gate_half, upstream, conv_taps, norm_gain, out_weight):
+    f32, bf16 = jnp.float32, jnp.bfloat16
+    nsp, ndp = lax.axis_size("sp"), lax.axis_size("dp")
+    nz = ndp // 2
+    _, length, channels = value_half.shape
+    rows = out_weight.shape[0]
+    tap_count, width = conv_taps.shape
+    halo = (tap_count - 1 + 15) // 16 * 16
+    half, side, share = channels // 2, channels // 4, 2 * rows // nsp
+    tap_rows = (tap_count + 8) // 8 * 8
+
+    def shape(*dims, dtype=bf16):
+        return jax.ShapeDtypeStruct(dims, dtype)
+
+    def vmem(*dims, dtype=bf16):
+        return pltpu.VMEM(dims, dtype)
+
+    any_space = pl.BlockSpec(memory_space=pl.ANY)
+    remote = 60 + 30 * nz
+    grad_value, grad_gate, grad_taps, grad_gain, grad_weight = pl.pallas_call(
+        fused,
+        out_shape=[
+            shape(length, channels),
+            shape(length, channels),
+            shape(tap_count, width, dtype=f32),
+            shape(1, channels, dtype=f32),
+            shape(rows, channels, dtype=f32),
+        ],
+        in_specs=[any_space] * 6,
+        out_specs=[VMEM] * 5,
+        scratch_shapes=[
+            vmem(length, channels),
+            vmem(length, channels),
+            vmem(2 * length, channels),
+            vmem(nsp, tap_count, width, dtype=f32),
+            vmem(1, channels, dtype=f32),
+            vmem(ndp * rows, channels),
+            vmem(halo, channels),
+            vmem(halo, channels),
+            vmem(length + halo, channels, dtype=f32),
+            vmem(length, channels, dtype=f32),
+            vmem(length, LANES, dtype=f32),
+            vmem(2 * length, half),
+            vmem(length, channels),
+            vmem(nz, 2 * rows, half),
+            vmem(nz, 2, share, side),
+            vmem(nz, 2, share, side),
+            vmem(nz, share, side),
+            vmem(nz, share, side),
+            vmem(nz, share, half),
+            vmem(nz, share, half),
+            vmem(2 * rows, half),
+            vmem(rows, half),
+            vmem(nz, share, side),
+            vmem(nz, share, side),
+            vmem(length, channels, dtype=f32),
+            vmem(halo, channels),
+            vmem(halo, channels),
+            vmem(length + halo, channels, dtype=f32),
+            vmem(tap_count, 8, channels, dtype=f32),
+            vmem(8, channels, dtype=f32),
+            vmem(nsp, tap_rows, width, dtype=f32),
+            vmem(nsp, tap_rows, width, dtype=f32),
+            vmem(nz, tap_rows, width, dtype=f32),
+            vmem(tap_rows, width, dtype=f32),
+            vmem(tap_rows, width, dtype=f32),
+            vmem(tap_rows, width, dtype=f32),
+            vmem(nsp, 8, width, dtype=f32),
+            pltpu.SemaphoreType.DMA((remote,)),
+            pltpu.SemaphoreType.DMA((remote,)),
+            pltpu.SemaphoreType.DMA((8,)),
+        ],
+        compiler_params=pltpu.CompilerParams(
+            collective_id=7, has_side_effects=True, vmem_limit_bytes=60 * 1024 * 1024
+        ),
+    )(value_half, gate_half, upstream, conv_taps, norm_gain[None], out_weight)
+    return (grad_value[None], grad_gate[None], grad_taps, grad_gain[0], grad_weight)
+
+
 def solution(mesh):
     tokens = P("dp", "sp", None)
+    quarters = mesh.shape["sp"] == 4 and mesh.shape["dp"] >= 4
     return jax.shard_map(
-        body,
+        fused_body if quarters else body,
         mesh=mesh,
         in_specs=(tokens, tokens, tokens, P(None, "sp"), P(), P("dp", None)),
         out_specs=(tokens, tokens, P(None, "sp"), P(), P("dp", None)),

time: 237 us -> 127 us (0.54)
  the two profiles are of different devices: /device:TPU:1 before, /device:TPU:19 now
where the time goes in v1:
time: 127 us
  Pallas kernels  120 us (94%)
  local copies, waits for them, and re-layouts  5.99 us (5%)
    pallas_call x1, Pallas kernels, fused_body(): pl.pallas_call(fused, out_shape=[shape(length, channels), shape(length, c...  120 us
    unnamed x13, local copies, waits for them, and re-layouts  5.99 us

profile of v1, /device:TPU:19, one launch (start us, length us, event | category | flops | bytes accessed | tf_op | source)
XLA Modules:
  0.0 127.0 jit_solution(18021788973103883551)
XLA Ops:
  0.6 120.4 %shard_map.101 = (bf16[256,2048]{1,0:T(8,128)(2,1)}, bf16[256,2048]{1,0:T(8,128)(2,1)}, f32[31,512]{1,0:T(8,128)}, f32[1,2048]{1,0:T(1,128)}, f32[256,2048]{1,0:T(8,128)}) custom-call(bf16[1,256,2048]{2,1,0:T(8,128)(2,1)} %value_hbm.1, bf16[1,256,2048]{2,1,0:T(8,128)(2,1)} %gate_hbm.1, bf16[1,256,2048]{2,1,0:T(8,128)(2,1)} %up_hbm.1, f32[31,512]{1,0:T(8,128)} %taps_hbm.1, ...), custom_call_target="tpu_custom_call" | custom-call | tf_op jit(solution)/shard_map/pallas_call | solution.py:861
  121.0 0.0 copy-start.1
  121.0 0.0 copy-start.2
  121.0 0.0 copy-start.3
  121.0 0.0 copy-start
  121.1 2.5 %copy.16 = bf16[1,256,2048]{2,1,0:T(8,128)(2,1)} copy(bf16[1,256,2048]{2,1,0:T(8,128)(2,1)} %bitcast.5) | data formatting | bytes 2097152
  123.5 0.0 copy-done.1
  123.5 1.0 copy.17
  124.5 0.0 copy-done.2
  124.5 0.6 copy.18
  125.1 0.0 copy-done.3
  125.1 0.6 copy.19
  125.7 0.0 copy-done
  125.7 1.3 %copy.20 = f32[256,2048]{1,0:T(8,128)} copy(f32[256,2048]{1,0:T(8,128)S(1)} %copy-done) | data formatting | bytes 4194304
Async XLA Ops:
  121.0 2.5 %copy-start.1 = (bf16[256,2048]{1,0:T(8,128)(2,1)S(1)}, bf16[256,2048]{1,0:T(8,128)(2,1)}, u32[]{:S(2)}) copy-start(bf16[256,2048]{1,0:T(8,128)(2,1)} %get-tuple-element.11) | copy-start | bytes 3145732
  121.0 3.5 %copy-start.2 = (f32[31,512]{1,0:T(8,128)S(1)}, f32[31,512]{1,0:T(8,128)}, u32[]{:S(2)}) copy-start(f32[31,512]{1,0:T(8,128)} %get-tuple-element.22) | copy-start | bytes 190468
  121.0 4.1 %copy-start.3 = (f32[1,2048]{1,0:T(1,128)S(1)}, f32[1,2048]{1,0:T(1,128)}, u32[]{:S(2)}) copy-start(f32[1,2048]{1,0:T(1,128)} %get-tuple-element.13) | copy-start | bytes 24580
  121.0 4.7 %copy-start = (f32[256,2048]{1,0:T(8,128)S(1)}, f32[256,2048]{1,0:T(8,128)}, u32[]{:S(2)}) copy-start(f32[256,2048]{1,0:T(8,128)} %get-tuple-element.24) | copy-start | bytes 6291460

commit v2 on v1

--- a/solution.py
+++ b/solution.py
@@ -367,8 +367,8 @@
             device_id=to,
             device_id_type=pl.DeviceIdType.MESH,
         )
-        copy.start()
-        self.open.append(copy)
+        when(sends, copy.start)
+        self.open.append((copy, sends))
         return copy
 
     def arrival(self, ref, slot, to):
@@ -388,8 +388,8 @@
         return copy
 
     def finish(self):
-        for copy in self.open:
-            copy.wait_send()
+        for copy, sends in self.open:
+            when(sends, copy.wait_send)
 
 
 def nearest(z, nz, i):
@@ -405,6 +405,7 @@
     grad_value, grad_gate, grad_taps, grad_gain, grad_weight,
     value, gate, ups, taps, gain, weight, tail, before, padded, conv, scale, acts, act,
     parts, got_x, got_y, got_xy, got_yx, plane, got_z, final, halves, give_x, give_y,
+    got_e, early, e_x, e_y, e_xy, e_yx, e_give_x, e_give_y,
     grad_act, head, after, grads, tap_sums, gain_sum, terms, got_terms, got_dp, row_part, both_parts,
     tap_other, gain_rows,
     send, recv, local,
@@ -422,7 +423,9 @@
     width = taps.shape[2]
     rows = weight.shape[0] // ndp
     half = channels // 2
-    side = half // 2
+    lead = got_e.shape[2]
+    rest = half - lead
+    side, e_side = rest // 2, lead // 2
     quarter = channels // nsp
     share = 2 * rows // nsp
     tiles = channels // LANES
@@ -455,18 +458,19 @@
             pl.ds(al(owner * rows + h * r, r), r), pl.ds(al(q * quarter, quarter), quarter)
         ]
 
-    hops = [(i, h) for i in range(nz - 1) for h in range(2)]
-    in_weight.wait()
-    w_slots = net.ids(2 * nz)
-    for i, h in hops:
-        peer = nearest(z, nz, i)
-        net.put(piece(d, s, h), piece(d, s, h), at_chip(peer), w_slots + 2 * z + h)
-    in_up.wait()
-    own_rows = weight.at[pl.ds(al(d * rows, rows), rows)]
-    own_weight = net.put(own_rows, own_rows, partner)
-    own_up = net.put(ups.at[pl.ds(0, length)], ups.at[pl.ds(length, length)], partner)
+    above, below = at_chip(lax.rem(z + 1, nz)), at_chip(lax.rem(z + nz - 1, nz))
+
+    def along(src, h):
+        p, slot = piece(2 * src + c, s, h), w_slots + 2 * src + h
+        net.put(p, p, above, slot, jnp.logical_and(src <= z, z < nz - 1))
+        net.put(p, p, below, slot, jnp.logical_and(src >= z, z > 0))
+
     in_taps.wait()
     tap_copies = [net.put(taps.at[s], taps.at[s], to) for to in (to_x, to_y, to_d)]
+    w_slots = net.ids(2 * nz)
+    in_weight.wait()
+    for h in range(2):
+        along(z, h)
 
     arrived = {}
     mates = {}
@@ -475,6 +479,7 @@
         src = nearest(z, nz, i)
         owner = 2 * src + c
         net.arrival(piece(owner, s, h), w_slots + 2 * src + h, partner)
+        along(src, h)
         p = piece(owner, s, h)
         arrived[i, h] = [net.put(p, p, to_x), net.put(p, p, to_y)]
         mates.setdefault(i, []).append(net.put(p, p, partner))
@@ -499,19 +504,6 @@
         p = piece(owner, dg, h)
         mates[i].append(net.put(p, p, partner))
 
-    weight_steps = []
-    for n in range(len(hops) + 2):
-        if n < len(hops):
-            weight_steps.append(functools.partial(first, *hops[n]))
-        if 1 <= n <= len(hops):
-            weight_steps.append(functools.partial(second, *hops[n - 1]))
-        if n >= 2:
-            weight_steps.append(functools.partial(third, *hops[n - 2]))
-
-    def gather_weight(count):
-        for _ in range(min(count, len(weight_steps))):
-            weight_steps.pop(0)()
-
     in_value.wait()
     in_gate.wait()
     v = value[length - halo :, :].astype(f32)
@@ -525,14 +517,24 @@
         return 0
 
     lax.fori_loop(0, 2, glu_rows, 0)
-    left = net.put(tail, before, {"sp": lax.rem(s + 1, nsp)})
+    left = net.put(tail, before, {"sp": lax.rem(s + 1, nsp)}, None, s < nsp - 1)
+    in_up.wait()
+    own_rows = weight.at[pl.ds(al(d * rows, rows), rows)]
+    own_up = net.put(ups.at[pl.ds(0, length)], ups.at[pl.ds(length, length)], partner)
+    own_weight = net.put(own_rows, own_rows, partner)
     lax.fori_loop(2, length // 16, glu_rows, 0)
-    gather_weight(1)
-    for copy in tap_copies:
-        copy.wait_recv()
-    left.wait_recv()
-    b = before[...].astype(f32)
-    padded[pl.ds(0, halo), :] = jnp.where(s == 0, jnp.zeros_like(b), b)
+
+    def tap_from(n):
+        tap_copies[n].wait_recv()
+
+    def left_halo():
+        when(s > 0, left.wait_recv)
+
+        @pl.when(s == 0)
+        def _():
+            before[...] = jnp.zeros_like(before)
+
+        padded[pl.ds(0, halo), :] = before[...].astype(f32)
 
     per_block = width // LANES
 
@@ -543,28 +545,37 @@
     def turned(window, r):
         return window if r == 0 else pltpu.roll(window, window.shape[0] - r, 0)
 
-    def conv_tile(t, _):
+    def conv_block(t, i):
         cols = pl.ds(al(t * LANES, LANES), LANES)
-
-        def block(i, _):
-            r0 = al(i * BLOCK, BLOCK)
-            window = padded[pl.ds(r0, BLOCK + halo), cols]
-            total = jnp.zeros((BLOCK, LANES), f32)
-            for r in range(8):
-                moved = turned(window, r)
-                for o in range(r, halo + 1, 8):
-                    j = o - (halo - tap_count + 1)
-                    if 0 <= j < tap_count:
-                        total = total + tap(t, j) * moved[o - r : o - r + BLOCK]
-            conv[pl.ds(r0, BLOCK), cols] = total.astype(bf16).astype(f32)
+        r0 = al(i * BLOCK, BLOCK)
+        window = padded[pl.ds(r0, BLOCK + halo), cols]
+        total = jnp.zeros((BLOCK, LANES), f32)
+        for r in range(8):
+            moved = turned(window, r)
+            for o in range(r, halo + 1, 8):
+                j = o - (halo - tap_count + 1)
+                if 0 <= j < tap_count:
+                    total = total + tap(t, j) * moved[o - r : o - r + BLOCK]
+        conv[pl.ds(r0, BLOCK), cols] = total.astype(bf16).astype(f32)
+
+    row_blocks = length // BLOCK
+
+    def conv_quarter(n):
+        q = (s, xn, yn, dg)[n]
+        inner = row_blocks - 1
+
+        def one(m, _):
+            conv_block(q * per_block + m // inner, 1 + lax.rem(m, inner))
             return 0
 
-        return lax.fori_loop(0, length // BLOCK, block, 0)
-
-    part = tiles // 4
-    for n in range(4):
-        lax.fori_loop(n * part, (n + 1) * part, conv_tile, 0)
-        gather_weight(1)
+        lax.fori_loop(0, per_block * inner, one, 0)
+
+    def conv_head(n):
+        def one(t, _):
+            conv_block(t, 0)
+            return 0
+
+        lax.fori_loop(n * tiles // 2, (n + 1) * tiles // 2, one, 0)
 
     in_gain.wait()
 
@@ -583,25 +594,24 @@
         return 0
 
     blocks = length // 16
-    lax.fori_loop(0, blocks // 2, norm_rows, 0)
-    gather_weight(1)
-    lax.fori_loop(blocks // 2, blocks, norm_rows, 0)
+
+    def norm(n):
+        lax.fori_loop(n * blocks // 4, (n + 1) * blocks // 4, norm_rows, 0)
 
     mine = pl.ds(al(c * half, half), half)
     other = pl.ds(al((1 - c) * half, half), half)
-    act_copy = net.put(act.at[:, other], acts.at[pl.ds(length, length)], partner)
-    acts[pl.ds(0, length), :] = act[:, mine]
-    gather_weight(2)
-    own_up.wait_recv()
-    act_copy.wait_recv()
+    swapped = []
+
+    def swap():
+        swapped.append(net.put(act.at[:, other], acts.at[pl.ds(length, length)], partner))
+        acts[pl.ds(0, length), :] = act[:, mine]
+
+    def swap_done():
+        own_up.wait_recv()
+        swapped[0].wait_recv()
 
     def target(k):
         return nearest(z, nz, nz - 2 - k) if k < nz - 1 else z
-
-    phase_one, phase_two = {}, {}
-
-    def unit(ref, q, h):
-        return ref.at[pl.ds(al(q * share, share), share), pl.ds(h * side, side)]
 
     def multiply(k):
         t = target(k)
@@ -615,48 +625,93 @@
 
         lax.fori_loop(0, 2 * rows // step, some, 0)
 
-    def scatter_one(k):
-        p = parts.at[k]
-        phase_one[k] = [
-            net.put(unit(p, dg, 0), got_x.at[k, 1], to_x),
-            net.put(unit(p, dg, 1), got_y.at[k, 1], to_y),
-            net.put(unit(p, xn, 0), got_x.at[k, 0], to_x),
-            net.put(unit(p, yn, 1), got_y.at[k, 0], to_y),
-        ]
-
-    def own(k, q, h):
-        return parts[k, pl.ds(al(q * share, share), share), pl.ds(h * side, side)].astype(f32)
-
-    def scatter_two(k):
-        diag_x, diag_y, mine_x, mine_y = phase_one[k]
-        diag_x.wait_recv()
-        give_y[k] = (own(k, yn, 0) + got_x[k, 1].astype(f32)).astype(bf16)
-        diag_y.wait_recv()
-        give_x[k] = (own(k, xn, 1) + got_y[k, 1].astype(f32)).astype(bf16)
-        phase_two[k] = [
-            net.put(give_y.at[k], got_xy.at[k], to_y),
-            net.put(give_x.at[k], got_yx.at[k], to_x),
-        ]
-        mine_x.wait_recv()
-        mine_y.wait_recv()
-
-    z_slots = net.ids(nz)
-
-    def scatter_three(k):
-        for copy in phase_two[k]:
-            copy.wait_recv()
-        low = own(k, s, 0) + got_x[k, 0].astype(f32) + got_xy[k].astype(f32)
-        high = own(k, s, 1) + got_y[k, 0].astype(f32) + got_yx[k].astype(f32)
-        plane[k, :, pl.ds(0, side)] = low.astype(bf16)
-        plane[k, :, pl.ds(side, side)] = high.astype(bf16)
+    class Plane:
+        def __init__(self, src, w, x, y, xy, yx, give_x, give_y):
+            self.src, self.w = src, w
+            self.x, self.y, self.xy, self.yx = x, y, xy, yx
+            self.give_x, self.give_y = give_x, give_y
+
+        def at(self, q, h):
+            return pl.ds(al(q * share, share), share), pl.ds(h * self.w, self.w)
+
+        def part(self, q, h):
+            return self.src[self.at(q, h)].astype(f32)
+
+        def send(self):
+            def unit(q, h):
+                return self.src.at[self.at(q, h)]
+
+            self.far_x = net.put(unit(dg, 0), self.x.at[1], to_x)
+            self.far_y = net.put(unit(dg, 1), self.y.at[1], to_y)
+            self.near_x = net.put(unit(xn, 0), self.x.at[0], to_x)
+            self.near_y = net.put(unit(yn, 1), self.y.at[0], to_y)
+
+        def turn_x(self):
+            self.far_x.wait_recv()
+            self.give_y[...] = (self.part(yn, 0) + self.x[1].astype(f32)).astype(bf16)
+            self.last_y = net.put(self.give_y, self.xy, to_y)
+
+        def turn_y(self):
+            self.far_y.wait_recv()
+            self.give_x[...] = (self.part(xn, 1) + self.y[1].astype(f32)).astype(bf16)
+            self.last_x = net.put(self.give_x, self.yx, to_x)
+
+        def total(self):
+            for copy in (self.near_x, self.near_y, self.last_x, self.last_y):
+                copy.wait_recv()
+            low = self.part(s, 0) + self.x[0].astype(f32) + self.xy[...].astype(f32)
+            high = self.part(s, 1) + self.y[0].astype(f32) + self.yx[...].astype(f32)
+            return low.astype(bf16), high.astype(bf16)
+
+    chunks = [
+        Plane(
+            parts.at[k], side, got_x.at[k], got_y.at[k], got_xy.at[k], got_yx.at[k],
+            give_x.at[k], give_y.at[k],
+        )
+        for k in range(nz)
+    ]
+    ahead = Plane(early, e_side, e_x, e_y, e_xy, e_yx, e_give_x, e_give_y)
+    z_slots, e_slots = net.ids(nz), net.ids(nz)
+
+    def load(k):
+        chunks[k].send()
+
+    def turn_x(k):
+        chunks[k].turn_x()
+
+    def turn_y(k):
+        chunks[k].turn_y()
+
+    def hand_on(k):
+        low, high = chunks[k].total()
+        plane[k, :, pl.ds(0, side)] = low
+        plane[k, :, pl.ds(side, side)] = high
         if k < nz - 1:
             net.put(plane.at[k], got_z.at[z], at_chip(target(k)), z_slots + z)
 
-    multiply(0)
-    gather_weight(2)
-    scatter_one(0)
-    multiply(1)
-    gather_weight(2)
+    def send_early(k):
+        if k < nz - 1:
+            tops = parts.at[k, :, pl.ds(rest, lead)]
+            net.put(tops, got_e.at[z], at_chip(target(k)), e_slots + z)
+
+    def add_early():
+        total = parts[nz - 1, :, pl.ds(rest, lead)].astype(f32)
+        for i in range(nz - 1):
+            src = nearest(z, nz, i)
+            net.arrival(got_e.at[src], e_slots + src, partner)
+            total = total + got_e[src].astype(f32)
+        early[...] = total.astype(bf16)
+        ahead.send()
+
+    def turn_early():
+        ahead.turn_x()
+        ahead.turn_y()
+
+    def keep_early():
+        low, high = ahead.total()
+        own = pl.ds(al(s * share, share), share)
+        final[own, pl.ds(rest, e_side)] = low
+        final[own, pl.ds(rest + e_side, e_side)] = high
 
     def product(owner, start):
         w = weight[pl.ds(al(owner * rows, rows), rows), :]
@@ -664,33 +719,24 @@
         p = jnp.dot(u, w, preferred_element_type=f32)
         grad_act[...] = p if start else grad_act[...] + p
 
-    product(d, True)
-    own_weight.wait_recv()
-
-    def blocks_of(src):
-        def one(i, _):
-            product(2 * src + i, False)
-            return 0
-
-        lax.fori_loop(0, 2, one, 0)
-
-    product(d + 1 - 2 * c, False)
-    gather_weight(2)
-    scatter_one(1)
-    multiply(2)
-    gather_weight(2)
-    for i in range(nz - 1):
-        gather_weight(2 if i < nz - 2 else len(weight_steps))
-        if i == nz - 2:
-            scatter_one(2)
-            multiply(3)
+    def product_own():
+        product(d, True)
+
+    def product_mate():
+        own_weight.wait_recv()
+        product(d + 1 - 2 * c, False)
+
+    def blocks_of(i):
+        assert len(mates[i]) == 8
         for copy in mates[i]:
             copy.wait_recv()
-        blocks_of(nearest(z, nz, i))
-    for k in range(3, nz):
-        if k > 3:
-            multiply(k)
-        scatter_one(k)
+        src = nearest(z, nz, i)
+
+        def one(n, _):
+            product(2 * src + n, False)
+            return 0
+
+        lax.fori_loop(0, 2, one, 0)
 
     gain_sum[...] = jnp.zeros_like(gain_sum)
 
@@ -710,132 +756,244 @@
         grads[rr, :] = gc.astype(f32)
         return 0
 
-    lax.fori_loop(0, halo // 16, back_rows, 0)
-    head[...] = grads[pl.ds(0, halo), :].astype(bf16)
-    scatter_two(0)
-    right = net.put(head, after, {"sp": lax.rem(s + nsp - 1, nsp)})
-    lax.fori_loop(halo // 16, blocks // 2, back_rows, 0)
-    scatter_three(0)
-    lax.fori_loop(blocks // 2, blocks, back_rows, 0)
-    scatter_two(1)
-    right.wait_recv()
-    a = after[...].astype(f32)
-    grads[pl.ds(length, halo), :] = jnp.where(s == nsp - 1, jnp.zeros_like(a), a)
+    ready = []
+
+    def back_head():
+        lax.fori_loop(0, halo // 16, back_rows, 0)
+        head[...] = grads[pl.ds(0, halo), :].astype(bf16)
+        ready.append(net.put(head, after, {"sp": lax.rem(s + nsp - 1, nsp)}, None, s > 0))
+
+    def back(n):
+        mid = (blocks + halo // 16) // 2
+        lax.fori_loop((halo // 16, mid)[n], (mid, blocks)[n], back_rows, 0)
+
+    def right_halo():
+        when(s < nsp - 1, ready[0].wait_recv)
+
+        @pl.when(s == nsp - 1)
+        def _():
+            after[...] = jnp.zeros_like(after)
+
+        grads[pl.ds(length, halo), :] = after[...].astype(f32)
 
     tap_sums[...] = jnp.zeros_like(tap_sums)
 
-    def back_tile(t, _):
+    def back_block(t, i):
         cols = pl.ds(al(t * LANES, LANES), LANES)
-
-        def block(i, _):
-            r0 = al(i * BLOCK, BLOCK)
-            rr = pl.ds(r0, BLOCK)
-            window = grads[pl.ds(r0, BLOCK + halo), cols]
-            total = jnp.zeros((BLOCK, LANES), f32)
-            for r in range(8):
-                moved = turned(window, r)
-                for o in range(r, tap_count, 8):
-                    total = total + tap(t, tap_count - 1 - o) * moved[o - r : o - r + BLOCK]
-            gg = total.astype(bf16).astype(f32)
-            sg = jax.nn.sigmoid(gate[rr, cols].astype(f32))
-            grad_value[rr, cols] = (gg * sg).astype(bf16)
-            grad_gate[rr, cols] = (gg * value[rr, cols].astype(f32) * sg * (1.0 - sg)).astype(bf16)
-            gc = window[:BLOCK]
-            window = padded[pl.ds(r0, BLOCK + halo), cols]
-            for r in range(8):
-                moved = turned(window, r)
-                for o in range(r, halo + 1, 8):
-                    j = o - (halo - tap_count + 1)
-                    if 0 <= j < tap_count:
-                        term = (gc * moved[o - r : o - r + BLOCK]).reshape(BLOCK // 8, 8, LANES)
-                        tap_sums[j, :, cols] += jnp.sum(term, axis=0)
+        r0 = al(i * BLOCK, BLOCK)
+        rr = pl.ds(r0, BLOCK)
+        window = grads[pl.ds(r0, BLOCK + halo), cols]
+        total = jnp.zeros((BLOCK, LANES), f32)
+        for r in range(8):
+            moved = turned(window, r)
+            for o in range(r, tap_count, 8):
+                total = total + tap(t, tap_count - 1 - o) * moved[o - r : o - r + BLOCK]
+        gg = total.astype(bf16).astype(f32)
+        sg = jax.nn.sigmoid(gate[rr, cols].astype(f32))
+        grad_value[rr, cols] = (gg * sg).astype(bf16)
+        grad_gate[rr, cols] = (gg * value[rr, cols].astype(f32) * sg * (1.0 - sg)).astype(bf16)
+        gc = window[:BLOCK]
+        window = padded[pl.ds(r0, BLOCK + halo), cols]
+        for r in range(8):
+            moved = turned(window, r)
+            for o in range(r, halo + 1, 8):
+                j = o - (halo - tap_count + 1)
+                if 0 <= j < tap_count:
+                    term = (gc * moved[o - r : o - r + BLOCK]).reshape(BLOCK // 8, 8, LANES)
+                    tap_sums[j, :, cols] += jnp.sum(term, axis=0)
+
+    def back_tiles(n):
+        inner = row_blocks - 1
+
+        def one(m, _):
+            back_block(m // inner, lax.rem(m, inner))
             return 0
 
-        lax.fori_loop(0, length // BLOCK, block, 0)
-        q, lane = t // per_block, lax.rem(t, per_block)
-        lanes = pl.ds(al(lane * LANES, LANES), LANES)
-        terms[q, pl.ds(0, tap_count), lanes] = jnp.sum(tap_sums[:, :, cols], axis=1)
-        return 0
-
-    order = []
-    for k in range(nz):
-        if k >= 1:
-            order.append(functools.partial(scatter_three, k))
-        if k + 2 <= nz - 1:
-            order.append(functools.partial(scatter_two, k + 2))
-    pieces = 8
-    part = tiles // pieces
-    for n in range(pieces):
-        lax.fori_loop(n * part, (n + 1) * part, back_tile, 0)
-        if n >= 2 and order:
-            order.pop(0)()
-    for q in range(nsp):
-        total = jnp.sum(gain_sum[:, pl.ds(q * width, width)], axis=0, keepdims=True)
-        terms[q, pl.ds(tap_count, 1), :] = total
-    scattered = [
-        net.put(terms.at[peer], got_terms.at[s], to)
-        for peer, to in ((dg, to_d), (xn, to_x), (yn, to_y))
-    ]
-    while order:
-        order.pop(0)()
-    got_terms[s] = terms[s]
-    for copy in scattered:
-        copy.wait_recv()
-    total = got_terms[0]
-    for q in range(1, nsp):
-        total = total + got_terms[q]
-    row_part[...] = total
-    got_dp[z] = total
+        step = tiles // 8 * inner
+        lax.fori_loop(n * step, (n + 1) * step, one, 0)
+
+    def back_tail(n):
+        def one(t, _):
+            back_block(t, row_blocks - 1)
+            cols = pl.ds(al(t * LANES, LANES), LANES)
+            q, lane = t // per_block, lax.rem(t, per_block)
+            lanes = pl.ds(al(lane * LANES, LANES), LANES)
+            terms[q, pl.ds(0, tap_count), lanes] = jnp.sum(tap_sums[:, :, cols], axis=1)
+            return 0
+
+        lax.fori_loop(n * tiles // 2, (n + 1) * tiles // 2, one, 0)
+
+    sums = {}
+
+    def send_terms():
+        for q in range(nsp):
+            total = jnp.sum(gain_sum[:, pl.ds(q * width, width)], axis=0, keepdims=True)
+            terms[q, pl.ds(tap_count, 1), :] = total
+        sums["sp"] = [
+            net.put(terms.at[peer], got_terms.at[s], to)
+            for peer, to in ((dg, to_d), (xn, to_x), (yn, to_y))
+        ]
+        got_terms[s] = terms[s]
+
     tap_slots = net.ids(nz)
-    for i in range(nz - 1):
-        net.put(row_part, got_dp.at[z], at_chip(nearest(z, nz, i)), tap_slots + z)
-
-    for i in range(nz - 1):
-        src = nearest(z, nz, i)
-        net.arrival(got_z.at[src], z_slots + src, partner)
-    total = plane[nz - 1].astype(f32)
-    for i in range(nz - 1):
-        total = total + got_z[nearest(z, nz, i)].astype(f32)
-    final[pl.ds(al(s * share, share), share), :] = total.astype(bf16)
+
+    def add_terms():
+        for copy in sums["sp"]:
+            copy.wait_recv()
+        total = got_terms[0]
+        for q in range(1, nsp):
+            total = total + got_terms[q]
+        row_part[...] = total
+        got_dp[z] = total
+        for i in range(nz - 1):
+            net.put(row_part, got_dp.at[z], at_chip(nearest(z, nz, i)), tap_slots + z)
 
     def done(q, h):
-        return unit(final, q, h)
-
-    sent = {
-        (axis, h): net.put(done(s, h), done(s, h), to_x if axis == "x" else to_y)
-        for axis, h in (("x", 0), ("y", 1), ("y", 0), ("x", 1))
-    }
-    for i in range(nz - 1):
-        src = nearest(z, nz, i)
-        net.arrival(got_dp.at[src], tap_slots + src, partner)
-    total = got_dp[0]
-    for i in range(1, nz):
-        total = total + got_dp[i]
-    both_parts[...] = total
-    tap_pair = net.put(both_parts, tap_other, partner)
-    sent["x", 0].wait_recv()
-    low = net.put(done(xn, 0), done(xn, 0), to_y)
-    sent["y", 1].wait_recv()
-    high = net.put(done(yn, 1), done(yn, 1), to_x)
-    tap_pair.wait_recv()
-    total = both_parts[...] + tap_other[...]
-    grad_taps[...] = total[:tap_count]
-    gain_rows[s] = total[total.shape[0] - 8 :]
-    gains = [net.put(gain_rows.at[s], gain_rows.at[s], to) for to in (to_d, to_x, to_y)]
-    sent["y", 0].wait_recv()
-    sent["x", 1].wait_recv()
-    low.wait_recv()
-    high.wait_recv()
+        return final.at[pl.ds(al(q * share, share), share), pl.ds(h * half // 2, half // 2)]
+
+    sent = {}
+
+    def finish_rows():
+        total = plane[nz - 1].astype(f32)
+        for i in range(nz - 1):
+            src = nearest(z, nz, i)
+            net.arrival(got_z.at[src], z_slots + src, partner)
+            total = total + got_z[src].astype(f32)
+        final[pl.ds(al(s * share, share), share), pl.ds(0, rest)] = total.astype(bf16)
+        for axis, h in (("x", 0), ("y", 1), ("y", 0), ("x", 1)):
+            sent[axis, h] = net.put(done(s, h), done(s, h), to_x if axis == "x" else to_y)
+
+    def pair_terms():
+        for i in range(nz - 1):
+            src = nearest(z, nz, i)
+            net.arrival(got_dp.at[src], tap_slots + src, partner)
+        total = got_dp[0]
+        for i in range(1, nz):
+            total = total + got_dp[i]
+        both_parts[...] = total
+        sums["pair"] = net.put(both_parts, tap_other, partner)
+
+    def spread_rows():
+        sent.pop(("x", 0)).wait_recv()
+        sent["low"] = net.put(done(xn, 0), done(xn, 0), to_y)
+        sent.pop(("y", 1)).wait_recv()
+        sent["high"] = net.put(done(yn, 1), done(yn, 1), to_x)
+
+    def keep_taps():
+        sums["pair"].wait_recv()
+        total = both_parts[...] + tap_other[...]
+        grad_taps[...] = total[:tap_count]
+        gain_rows[s] = total[total.shape[0] - 8 :]
+        sums["gain"] = [net.put(gain_rows.at[s], gain_rows.at[s], to) for to in (to_d, to_x, to_y)]
+
     mine_rows = pl.ds(al(c * rows, rows), rows)
     other_rows = pl.ds(al((1 - c) * rows, rows), rows)
-    last = net.put(final.at[other_rows], halves, partner)
-    grad_weight[:, mine] = final[mine_rows, :].astype(f32)
-    for copy in gains:
-        copy.wait_recv()
-    for q in range(nsp):
-        grad_gain[:, pl.ds(q * width, width)] = gain_rows[q][at_row : at_row + 1]
-    last.wait_recv()
-    grad_weight[:, other] = halves[...].astype(f32)
+
+    def gather_rows():
+        for copy in sent.values():
+            copy.wait_recv()
+        sums["last"] = net.put(final.at[other_rows], halves, partner)
+        grad_weight[:, mine] = final[mine_rows, :].astype(f32)
+
+    def keep():
+        for copy in sums["gain"]:
+            copy.wait_recv()
+        for q in range(nsp):
+            grad_gain[:, pl.ds(q * width, width)] = gain_rows[q][at_row : at_row + 1]
+        sums["last"].wait_recv()
+        grad_weight[:, other] = halves[...].astype(f32)
+
+    for step, *at in (
+        (tap_from, 1),
+        (conv_quarter, 0),
+        (first, 0, 0),
+        (conv_quarter, 2),
+        (tap_from, 2),
+        (tap_from, 0),
+        (conv_quarter, 3),
+        (first, 0, 1),
+        (first, 1, 0),
+        (conv_quarter, 1),
+        (first, 1, 1),
+        (left_halo,),
+        (norm, 2),
+        (product_own,),
+        (second, 0, 0),
+        (conv_head, 1),
+        (first, 2, 0),
+        (norm, 3),
+        (second, 0, 1),
+        (conv_head, 0),
+        (norm, 0),
+        (norm, 1),
+        (product_mate,),
+        (swap,),
+        (first, 2, 1),
+        (second, 1, 0),
+        (swap_done,),
+        (third, 0, 0),
+        (multiply, 0),
+        (send_early, 0),
+        (third, 0, 1),
+        (second, 1, 1),
+        (second, 2, 0),
+        (multiply, 2),
+        (multiply, 3),
+        (second, 2, 1),
+        (multiply, 1),
+        (load, 0),
+        (send_early, 1),
+        (third, 1, 0),
+        (load, 1),
+        (third, 1, 1),
+        (blocks_of, 0),
+        (blocks_of, 1),
+        (turn_y, 0),
+        (third, 2, 0),
+        (turn_x, 0),
+        (third, 2, 1),
+        (blocks_of, 2),
+        (send_early, 2),
+        (back_head,),
+        (back, 0),
+        (back, 1),
+        (back_tiles, 0),
+        (back_tiles, 1),
+        (load, 2),
+        (hand_on, 0),
+        (back_tiles, 2),
+        (right_halo,),
+        (send_early, 3),
+        (back_tiles, 3),
+        (turn_y, 1),
+        (turn_x, 1),
+        (turn_y, 2),
+        (turn_x, 2),
+        (load, 3),
+        (back_tail, 0),
+        (add_early,),
+        (back_tiles, 4),
+        (hand_on, 1),
+        (back_tiles, 5),
+        (turn_y, 3),
+        (hand_on, 2),
+        (turn_x, 3),
+        (back_tiles, 6),
+        (turn_early,),
+        (back_tiles, 7),
+        (back_tail, 1),
+        (send_terms,),
+        (hand_on, 3),
+        (keep_early,),
+        (finish_rows,),
+        (add_terms,),
+        (spread_rows,),
+        (pair_terms,),
+        (keep_taps,),
+        (gather_rows,),
+        (keep,),
+    ):
+        step(*at)
     net.finish()
 
 
@@ -847,7 +1005,9 @@
     rows = out_weight.shape[0]
     tap_count, width = conv_taps.shape
     halo = (tap_count - 1 + 15) // 16 * 16
-    half, side, share = channels // 2, channels // 4, 2 * rows // nsp
+    half, share = channels // 2, 2 * rows // nsp
+    lead = half // 4
+    side, e_side = (half - lead) // 2, lead // 2
     tap_rows = (tap_count + 8) // 8 * 8
 
     def shape(*dims, dtype=bf16):
@@ -888,12 +1048,20 @@
             vmem(nz, 2, share, side),
             vmem(nz, share, side),
             vmem(nz, share, side),
-            vmem(nz, share, half),
-            vmem(nz, share, half),
+            vmem(nz, share, half - lead),
+            vmem(nz, share, half - lead),
             vmem(2 * rows, half),
             vmem(rows, half),
             vmem(nz, share, side),
             vmem(nz, share, side),
+            vmem(nz, 2 * rows, lead),
+            vmem(2 * rows, lead),
+            vmem(2, share, e_side),
+            vmem(2, share, e_side),
+            vmem(share, e_side),
+            vmem(share, e_side),
+            vmem(share, e_side),
+            vmem(share, e_side),
             vmem(length, channels, dtype=f32),
             vmem(halo, channels),
             vmem(halo, channels),
@@ -920,7 +1088,7 @@
 
 def solution(mesh):
     tokens = P("dp", "sp", None)
-    quarters = mesh.shape["sp"] == 4 and mesh.shape["dp"] >= 4
+    quarters = mesh.shape["sp"] == 4 and mesh.shape["dp"] == 8
     return jax.shard_map(
         fused_body if quarters else body,
         mesh=mesh,

time: 127 us -> 96.9 us (0.76)
  the two profiles are of different devices: /device:TPU:19 before, /device:TPU:1 now
where the time goes in v2:
time: 96.9 us; the launch traced here: 96.4 us
  Pallas kernels  89.7 us (93%)
  local copies, waits for them, and re-layouts  5.99 us (6%)
    pallas_call x1, Pallas kernels, fused_body(): pl.pallas_call(fused, out_shape=[shape(length, channels), shape(length, c...  89.7 us
    unnamed x13, local copies, waits for them, and re-layouts  5.99 us

profile of v2, /device:TPU:1, one launch (start us, length us, event | category | flops | bytes accessed | tf_op | source)
XLA Modules:
  0.0 96.4 jit_solution(13691277296143510073)
XLA Ops:
  0.6 89.7 %shard_map.101 = (bf16[256,2048]{1,0:T(8,128)(2,1)}, bf16[256,2048]{1,0:T(8,128)(2,1)}, f32[31,512]{1,0:T(8,128)}, f32[1,2048]{1,0:T(1,128)}, f32[256,2048]{1,0:T(8,128)}) custom-call(bf16[1,256,2048]{2,1,0:T(8,128)(2,1)} %value_hbm.1, bf16[1,256,2048]{2,1,0:T(8,128)(2,1)} %gate_hbm.1, bf16[1,256,2048]{2,1,0:T(8,128)(2,1)} %up_hbm.1, f32[31,512]{1,0:T(8,128)} %taps_hbm.1, ...), custom_call_target="tpu_custom_call" | custom-call | tf_op jit(solution)/shard_map/pallas_call | solution.py:1021
  90.4 0.0 copy-start.1
  90.4 0.0 copy-start.2
  90.4 0.0 copy-start.3
  90.4 0.0 copy-start
  90.4 2.5 %copy.16 = bf16[1,256,2048]{2,1,0:T(8,128)(2,1)} copy(bf16[1,256,2048]{2,1,0:T(8,128)(2,1)} %bitcast.5) | data formatting | bytes 2097152
  92.9 0.0 copy-done.1
  92.9 1.0 %copy.17 = bf16[1,256,2048]{2,1,0:T(8,128)(2,1)} copy(bf16[1,256,2048]{2,1,0:T(8,128)(2,1)S(1)} %bitcast.4) | data formatting | bytes 2097152
  93.8 0.0 copy-done.2
  93.8 0.6 copy.18
  94.5 0.0 copy-done.3
  94.5 0.6 copy.19
  95.1 0.0 copy-done
  95.1 1.3 %copy.20 = f32[256,2048]{1,0:T(8,128)} copy(f32[256,2048]{1,0:T(8,128)S(1)} %copy-done) | data formatting | bytes 4194304
Async XLA Ops:
  90.4 2.5 %copy-start.1 = (bf16[256,2048]{1,0:T(8,128)(2,1)S(1)}, bf16[256,2048]{1,0:T(8,128)(2,1)}, u32[]{:S(2)}) copy-start(bf16[256,2048]{1,0:T(8,128)(2,1)} %get-tuple-element.11) | copy-start | bytes 3145732
  90.4 3.5 %copy-start.2 = (f32[31,512]{1,0:T(8,128)S(1)}, f32[31,512]{1,0:T(8,128)}, u32[]{:S(2)}) copy-start(f32[31,512]{1,0:T(8,128)} %get-tuple-element.22) | copy-start | bytes 190468
  90.4 4.1 %copy-start.3 = (f32[1,2048]{1,0:T(1,128)S(1)}, f32[1,2048]{1,0:T(1,128)}, u32[]{:S(2)}) copy-start(f32[1,2048]{1,0:T(1,128)} %get-tuple-element.13) | copy-start | bytes 24580
  90.4 4.7 %copy-start = (f32[256,2048]{1,0:T(8,128)S(1)}, f32[256,2048]{1,0:T(8,128)}, u32[]{:S(2)}) copy-start(f32[256,2048]{1,0:T(8,128)} %get-tuple-element.24) | copy-start | bytes 6291460

commit v3 on v2

--- a/solution.py
+++ b/solution.py
@@ -407,7 +407,7 @@
     parts, got_x, got_y, got_xy, got_yx, plane, got_z, final, halves, give_x, give_y,
     got_e, early, e_x, e_y, e_xy, e_yx, e_give_x, e_give_y,
     grad_act, head, after, grads, tap_sums, gain_sum, terms, got_terms, got_dp, row_part, both_parts,
-    tap_other, gain_rows,
+    tap_other, tap_mate, tap_half, gain_row, gain_mate, gain_pair, gain_sp, gain_part, gain_dp,
     send, recv, local,
 ):
     f32, bf16 = jnp.float32, jnp.bfloat16
@@ -429,7 +429,7 @@
     quarter = channels // nsp
     share = 2 * rows // nsp
     tiles = channels // LANES
-    at_row = tap_count - (terms.shape[1] - 8)
+    tap_rows, tap_width = terms.shape[2:]
     net = Net(send, recv, local)
     to_x, to_y, to_d, partner = {"sp": xn}, {"sp": yn}, {"sp": dg}, {"dp": d + 1 - 2 * c}
 
@@ -817,23 +817,58 @@
             back_block(t, row_blocks - 1)
             cols = pl.ds(al(t * LANES, LANES), LANES)
             q, lane = t // per_block, lax.rem(t, per_block)
+            e, lane = lane // (per_block // 2), lax.rem(lane, per_block // 2)
             lanes = pl.ds(al(lane * LANES, LANES), LANES)
-            terms[q, pl.ds(0, tap_count), lanes] = jnp.sum(tap_sums[:, :, cols], axis=1)
+            terms[e, q, pl.ds(0, tap_count), lanes] = jnp.sum(tap_sums[:, :, cols], axis=1)
             return 0
 
         lax.fori_loop(n * tiles // 2, (n + 1) * tiles // 2, one, 0)
 
     sums = {}
 
+    def send_gain():
+        gain_row[...] = jnp.sum(gain_sum[...], axis=0, keepdims=True)
+        sums["gain"] = net.put(gain_row, gain_mate, partner)
+
+    def pair_gain():
+        sums["gain"].wait_recv()
+        gain_pair[...] = gain_row[...] + gain_mate[...]
+        gain_sp[s] = gain_pair[...]
+        sums["gain"] = [net.put(gain_pair, gain_sp.at[s], to) for to in (to_d, to_x, to_y)]
+
+    gain_slots = net.ids(nz)
+
+    def line_gain():
+        for copy in sums["gain"]:
+            copy.wait_recv()
+        total = gain_sp[0]
+        for q in range(1, nsp):
+            total = total + gain_sp[q]
+        gain_part[...] = total
+        gain_dp[z] = total
+        for i in range(nz - 1):
+            net.put(gain_part, gain_dp.at[z], at_chip(nearest(z, nz, i)), gain_slots + z)
+
+    def keep_gain():
+        for i in range(nz - 1):
+            src = nearest(z, nz, i)
+            net.arrival(gain_dp.at[src], gain_slots + src, partner)
+        total = gain_dp[0]
+        for i in range(1, nz):
+            total = total + gain_dp[i]
+        grad_gain[...] = total
+
     def send_terms():
-        for q in range(nsp):
-            total = jnp.sum(gain_sum[:, pl.ds(q * width, width)], axis=0, keepdims=True)
-            terms[q, pl.ds(tap_count, 1), :] = total
+        sums["mate"] = net.put(terms.at[1 - c], tap_mate, partner)
+
+    def pair_sums():
+        sums["mate"].wait_recv()
+        tap_half[...] = terms[c] + tap_mate[...]
+        got_terms[s] = tap_half[s]
         sums["sp"] = [
-            net.put(terms.at[peer], got_terms.at[s], to)
+            net.put(tap_half.at[peer], got_terms.at[s], to)
             for peer, to in ((dg, to_d), (xn, to_x), (yn, to_y))
         ]
-        got_terms[s] = terms[s]
 
     tap_slots = net.ids(nz)
 
@@ -881,10 +916,9 @@
 
     def keep_taps():
         sums["pair"].wait_recv()
-        total = both_parts[...] + tap_other[...]
-        grad_taps[...] = total[:tap_count]
-        gain_rows[s] = total[total.shape[0] - 8 :]
-        sums["gain"] = [net.put(gain_rows.at[s], gain_rows.at[s], to) for to in (to_d, to_x, to_y)]
+        grad_taps[:, pl.ds(al(c * tap_width, tap_width), tap_width)] = both_parts[:tap_count]
+        theirs = pl.ds(al((1 - c) * tap_width, tap_width), tap_width)
+        grad_taps[:, theirs] = tap_other[:tap_count]
 
     mine_rows = pl.ds(al(c * rows, rows), rows)
     other_rows = pl.ds(al((1 - c) * rows, rows), rows)
@@ -896,105 +930,118 @@
         grad_weight[:, mine] = final[mine_rows, :].astype(f32)
 
     def keep():
-        for copy in sums["gain"]:
-            copy.wait_recv()
-        for q in range(nsp):
-            grad_gain[:, pl.ds(q * width, width)] = gain_rows[q][at_row : at_row + 1]
         sums["last"].wait_recv()
         grad_weight[:, other] = halves[...].astype(f32)
 
     for step, *at in (
         (tap_from, 1),
+        (tap_from, 0),
+        (product_own,),
         (conv_quarter, 0),
+        (tap_from, 2),
+        (conv_quarter, 3),
         (first, 0, 0),
-        (conv_quarter, 2),
-        (tap_from, 2),
-        (tap_from, 0),
-        (conv_quarter, 3),
         (first, 0, 1),
+        (left_halo,),
         (first, 1, 0),
         (conv_quarter, 1),
+        (conv_quarter, 2),
         (first, 1, 1),
-        (left_halo,),
+        (conv_head, 0),
+        (first, 2, 0),
+        (conv_head, 1),
+        (second, 0, 0),
         (norm, 2),
-        (product_own,),
-        (second, 0, 0),
-        (conv_head, 1),
-        (first, 2, 0),
+        (norm, 0),
+        (second, 0, 1),
+        (norm, 1),
         (norm, 3),
-        (second, 0, 1),
-        (conv_head, 0),
-        (norm, 0),
-        (norm, 1),
+        (first, 2, 1),
+        (swap,),
+        (second, 1, 0),
+        (second, 1, 1),
+        (swap_done,),
+        (multiply, 0),
+        (multiply, 1),
         (product_mate,),
-        (swap,),
-        (first, 2, 1),
-        (second, 1, 0),
-        (swap_done,),
+        (send_early, 0),
+        (second, 2, 0),
+        (second, 2, 1),
         (third, 0, 0),
-        (multiply, 0),
-        (send_early, 0),
         (third, 0, 1),
-        (second, 1, 1),
-        (second, 2, 0),
+        (third, 1, 0),
+        (third, 1, 1),
+        (send_early, 1),
+        (load, 0),
+        (load, 1),
         (multiply, 2),
+        (blocks_of, 0),
+        (turn_x, 0),
+        (turn_y, 0),
+        (blocks_of, 1),
+        (load, 2),
+        (third, 2, 0),
         (multiply, 3),
-        (second, 2, 1),
-        (multiply, 1),
-        (load, 0),
-        (send_early, 1),
-        (third, 1, 0),
-        (load, 1),
-        (third, 1, 1),
-        (blocks_of, 0),
-        (blocks_of, 1),
-        (turn_y, 0),
-        (third, 2, 0),
-        (turn_x, 0),
         (third, 2, 1),
+        (send_early, 2),
         (blocks_of, 2),
-        (send_early, 2),
+        (send_early, 3),
+        (turn_x, 1),
+        (turn_y, 1),
         (back_head,),
         (back, 0),
         (back, 1),
         (back_tiles, 0),
+        (hand_on, 0),
         (back_tiles, 1),
-        (load, 2),
-        (hand_on, 0),
+        (turn_x, 2),
+        (turn_y, 2),
         (back_tiles, 2),
+        (send_gain,),
+        (add_early,),
+        (back_tiles, 3),
+        (hand_on, 1),
+        (back_tiles, 4),
+        (back_tiles, 5),
         (right_halo,),
-        (send_early, 3),
-        (back_tiles, 3),
-        (turn_y, 1),
-        (turn_x, 1),
-        (turn_y, 2),
-        (turn_x, 2),
         (load, 3),
         (back_tail, 0),
-        (add_early,),
-        (back_tiles, 4),
-        (hand_on, 1),
-        (back_tiles, 5),
+        (hand_on, 2),
+        (back_tiles, 6),
+        (back_tiles, 7),
         (turn_y, 3),
-        (hand_on, 2),
         (turn_x, 3),
-        (back_tiles, 6),
+        (back_tail, 1),
         (turn_early,),
-        (back_tiles, 7),
-        (back_tail, 1),
         (send_terms,),
+        (pair_sums,),
+        (pair_gain,),
         (hand_on, 3),
         (keep_early,),
         (finish_rows,),
         (add_terms,),
+        (line_gain,),
         (spread_rows,),
         (pair_terms,),
+        (gather_rows,),
+        (keep_gain,),
         (keep_taps,),
-        (gather_rows,),
         (keep,),
     ):
         step(*at)
     net.finish()
+
+
+def write_out(*refs):
+    held, outs, sems = refs[:5], refs[5:10], refs[10]
+    copies = [
+        pltpu.make_async_copy(a, b.at[0] if len(b.shape) > len(a.shape) else b, sems.at[i])
+        for i, (a, b) in enumerate(zip(held, outs))
+    ]
+    for copy in copies:
+        copy.start()
+    for copy in copies:
+        copy.wait()
 
 
 def fused_body(value_half, gate_half, upstream, conv_taps, norm_gain, out_weight):
@@ -1008,7 +1055,7 @@
     half, share = channels // 2, 2 * rows // nsp
     lead = half // 4
     side, e_side = (half - lead) // 2, lead // 2
-    tap_rows = (tap_count + 8) // 8 * 8
+    tap_rows = (tap_count + 7) // 8 * 8
 
     def shape(*dims, dtype=bf16):
         return jax.ShapeDtypeStruct(dims, dtype)
@@ -1016,18 +1063,18 @@
     def vmem(*dims, dtype=bf16):
         return pltpu.VMEM(dims, dtype)
 
-    any_space = pl.BlockSpec(memory_space=pl.ANY)
+    hbm = pl.BlockSpec(memory_space=pltpu.MemorySpace.HBM)
     remote = 60 + 30 * nz
-    grad_value, grad_gate, grad_taps, grad_gain, grad_weight = pl.pallas_call(
+    results = pl.pallas_call(
         fused,
         out_shape=[
-            shape(length, channels),
-            shape(length, channels),
-            shape(tap_count, width, dtype=f32),
-            shape(1, channels, dtype=f32),
-            shape(rows, channels, dtype=f32),
+            vmem(length, channels),
+            vmem(length, channels),
+            vmem(tap_count, width, dtype=f32),
+            vmem(1, channels, dtype=f32),
+            vmem(rows, channels, dtype=f32),
         ],
-        in_specs=[any_space] * 6,
+        in_specs=[hbm] * 6,
         out_specs=[VMEM] * 5,
         scratch_shapes=[
             vmem(length, channels),
@@ -1068,22 +1115,43 @@
             vmem(length + halo, channels, dtype=f32),
             vmem(tap_count, 8, channels, dtype=f32),
             vmem(8, channels, dtype=f32),
-            vmem(nsp, tap_rows, width, dtype=f32),
-            vmem(nsp, tap_rows, width, dtype=f32),
-            vmem(nz, tap_rows, width, dtype=f32),
-            vmem(tap_rows, width, dtype=f32),
-            vmem(tap_rows, width, dtype=f32),
-            vmem(tap_rows, width, dtype=f32),
-            vmem(nsp, 8, width, dtype=f32),
+            vmem(2, nsp, tap_rows, width // 2, dtype=f32),
+            vmem(nsp, tap_rows, width // 2, dtype=f32),
+            vmem(nz, tap_rows, width // 2, dtype=f32),
+            vmem(tap_rows, width // 2, dtype=f32),
+            vmem(tap_rows, width // 2, dtype=f32),
+            vmem(tap_rows, width // 2, dtype=f32),
+            vmem(nsp, tap_rows, width // 2, dtype=f32),
+            vmem(nsp, tap_rows, width // 2, dtype=f32),
+            vmem(1, channels, dtype=f32),
+            vmem(1, channels, dtype=f32),
+            vmem(1, channels, dtype=f32),
+            vmem(nsp, 1, channels, dtype=f32),
+            vmem(1, channels, dtype=f32),
+            vmem(nz, 1, channels, dtype=f32),
             pltpu.SemaphoreType.DMA((remote,)),
             pltpu.SemaphoreType.DMA((remote,)),
             pltpu.SemaphoreType.DMA((8,)),
         ],
         compiler_params=pltpu.CompilerParams(
-            collective_id=7, has_side_effects=True, vmem_limit_bytes=60 * 1024 * 1024
+            collective_id=7, has_side_effects=True, vmem_limit_bytes=58 * 1024 * 1024
         ),
     )(value_half, gate_half, upstream, conv_taps, norm_gain[None], out_weight)
-    return (grad_value[None], grad_gate[None], grad_taps, grad_gain[0], grad_weight)
+    grad_value, grad_gate, grad_taps, grad_gain, grad_weight = pl.pallas_call(
+        write_out,
+        out_shape=[
+            shape(1, length, channels),
+            shape(1, length, channels),
+            shape(tap_count, width, dtype=f32),
+            shape(1, channels, dtype=f32),
+            shape(rows, channels, dtype=f32),
+        ],
+        in_specs=[VMEM] * 5,
+        out_specs=[hbm] * 5,
+        scratch_shapes=[pltpu.SemaphoreType.DMA((5,))],
+        compiler_params=pltpu.CompilerParams(vmem_limit_bytes=8 * 1024 * 1024),
+    )(*results)
+    return (grad_value, grad_gate, grad_taps, grad_gain[0], grad_weight)
 
 
 def solution(mesh):

time: 96.9 us -> 87.9 us (0.907)
  local copies, waits for them, and re-layouts: 5.99 us -> 0 us
  Pallas kernels: 89.7 us -> 87.1 us
    unnamed x13 -> x0, local copies, waits for them, and re-layouts: 5.99 us -> none
    pallas_call x1 -> x2, Pallas kernels: 89.7 us -> 87.1 us  [the longest x1 85 us: fused_body(): pl.pallas_call(fused, out_shape=[vmem(length, channels), vmem(length, cha...]
where the time goes in v3:
time: 87.9 us; the launch traced here: 87.8 us
  Pallas kernels  87.1 us (99%)
    pallas_call x1, Pallas kernels, fused_body(): pl.pallas_call(fused, out_shape=[vmem(length, channels), vmem(length, cha...  85 us
    pallas_call x1, Pallas kernels, fused_body(): pl.pallas_call(write_out, out_shape=[shape(1, length, channels), shape(1,...  2.08 us

profile of v3, /device:TPU:1, one launch (start us, length us, event | category | flops | bytes accessed | tf_op | source)
XLA Modules:
  0.0 87.8 jit_solution(5650270126619264667)
XLA Ops:
  0.6 85.0 %shard_map.101 = (bf16[256,2048]{1,0:T(8,128)(2,1)S(1)}, bf16[256,2048]{1,0:T(8,128)(2,1)S(1)}, f32[31,512]{1,0:T(8,128)S(1)}, f32[1,2048]{1,0:T(1,128)S(1)}, f32[256,2048]{1,0:T(8,128)S(1)}) custom-call(bf16[1,256,2048]{2,1,0:T(8,128)(2,1)} %value_hbm.1, bf16[1,256,2048]{2,1,0:T(8,128)(2,1)} %gate_hbm.1, bf16[1,256,2048]{2,1,0:T(8,128)(2,1)} %up_hbm.1, ...), custom_call_target="tpu_custom_call" | custom-call | tf_op jit(solution)/shard_map/pallas_call | solution.py:1068
  85.7 2.1 %shard_map.102 = (bf16[1,256,2048]{2,1,0:T(8,128)(2,1)}, bf16[1,256,2048]{2,1,0:T(8,128)(2,1)}, f32[31,512]{1,0:T(8,128)}, f32[1,2048]{1,0:T(1,128)}, f32[256,2048]{1,0:T(8,128)}) custom-call(bf16[256,2048]{1,0:T(8,128)(2,1)S(1)} %get-tuple-element.15.refs_0_, bf16[256,2048]{1,0:T(8,128)(2,1)S(1)} %get-tuple-element.16.refs_1_, ...), custom_call_target="tpu_custom_call" | custom-call | tf_op jit(solution)/shard_map/pallas_call | solution.py:1140

commit v4 on v3

--- a/solution.py
+++ b/solution.py
@@ -349,26 +349,32 @@
 class Net:
     def __init__(self, send, recv, local):
         self.send, self.recv, self.local = send, recv, local
-        self.n = self.m = 0
+        self.n = self.m = self.sends = 0
+        self.free = []
         self.open = []
-        self.landing = []
 
     def ids(self, count):
         self.n += count
         return self.n - count
 
+    def sender(self):
+        if self.free:
+            return self.free.pop(0)
+        self.sends += 1
+        return self.sends - 1
+
     def put(self, src, dst, to, slot=None, sends=None):
-        i = self.ids(1)
+        i = self.sender()
         copy = pltpu.make_async_remote_copy(
             src_ref=src,
             dst_ref=dst,
             send_sem=self.send.at[i],
-            recv_sem=self.recv.at[i if slot is None else slot],
+            recv_sem=self.recv.at[self.ids(1) if slot is None else slot],
             device_id=to,
             device_id_type=pl.DeviceIdType.MESH,
         )
         when(sends, copy.start)
-        self.open.append((copy, sends))
+        self.open.append((copy, sends, i))
         return copy
 
     def arrival(self, ref, slot, to):
@@ -381,15 +387,17 @@
             device_id_type=pl.DeviceIdType.MESH,
         ).wait_recv()
 
-    def load(self, src, dst):
+    def load(self, src, dst, here=None):
         copy = pltpu.make_async_copy(src, dst, self.local.at[self.m])
         self.m += 1
-        copy.start()
-        return copy
-
-    def finish(self):
-        for copy, sends in self.open:
+        when(here, copy.start)
+        return copy if here is None else (copy, here)
+
+    def drain(self, keep=0):
+        while len(self.open) > keep:
+            copy, sends, i = self.open.pop(0)
             when(sends, copy.wait_send)
+            self.free.append(i)
 
 
 def nearest(z, nz, i):
@@ -402,9 +410,9 @@
 
 def fused(
     value_hbm, gate_hbm, up_hbm, taps_hbm, gain_hbm, weight_hbm,
-    grad_value, grad_gate, grad_taps, grad_gain, grad_weight,
-    value, gate, ups, taps, gain, weight, tail, before, padded, conv, scale, acts, act,
-    parts, got_x, got_y, got_xy, got_yx, plane, got_z, final, halves, give_x, give_y,
+    out_value, out_gate, out_taps, out_gain, final,
+    grad_value, grad_gate, grad_taps, grad_gain, value, gate, ups, taps, gain, weight, tail, before, padded, conv, scale, acts, act,
+    parts, got_x, got_y, got_xy, got_yx, plane, got_z, summed, give_x, give_y,
     got_e, early, e_x, e_y, e_xy, e_yx, e_give_x, e_give_y,
     grad_act, head, after, grads, tap_sums, gain_sum, terms, got_terms, got_dp, row_part, both_parts,
     tap_other, tap_mate, tap_half, gain_row, gain_mate, gain_pair, gain_sp, gain_part, gain_dp,
@@ -447,7 +455,8 @@
     in_gain = net.load(gain_hbm, gain)
 
     barrier = pltpu.get_barrier_semaphore()
-    peers = [to_x, to_y, to_d, partner] + [at_chip(lax.rem(z + k, nz)) for k in range(1, nz)]
+    cross = [{**to, **partner} for to in (to_x, to_y)]
+    peers = [to_x, to_y, to_d, partner] + cross + [at_chip(lax.rem(z + k, nz)) for k in range(1, nz)]
     for peer in peers:
         pl.semaphore_signal(barrier, inc=1, device_id=peer, device_id_type=pl.DeviceIdType.MESH)
     pl.semaphore_wait(barrier, len(peers))
@@ -707,11 +716,75 @@
         ahead.turn_x()
         ahead.turn_y()
 
+    written = []
+
+    keeper = s // (nsp // 2)
+    same = keeper == c
+
+    class Spread:
+        def __init__(self, low, w):
+            self.low, self.w, self.slots = low, w, net.ids(14)
+
+        def place(self, q, e, h, count=1):
+            r = al(lax.rem(q, nsp // 2) * share, share)
+            col = al(e * half + self.low + h * self.w, LANES)
+            return pl.ds(r, share), pl.ds(col, count * self.w)
+
+        def send(self):
+            def go(h, to, i, count=1):
+                src = summed.at[:, pl.ds(self.low + h * self.w, count * self.w)]
+                dst = final.at[self.place(s, c, h, count)]
+                skip = None if count == 1 else jnp.logical_not(same)
+                net.put(src, dst, to, self.slots + 2 * i + c, skip)
+
+            core = {"dp": 2 * z + keeper}
+            go(0, {**to_x, **core}, 0)
+            go(1, {**to_y, **core}, 3)
+            go(0, {**to_y, **core}, 2)
+            go(1, {**to_x, **core}, 1)
+            go(0, partner, 6, 2)
+
+            src = summed.at[:, pl.ds(self.low, 2 * self.w)]
+            written.append(net.load(src, final.at[self.place(s, c, 0, 2)], same))
+
+        def arrive(self, who, q, h, i):
+            @pl.when(who)
+            def _():
+                for e in range(2):
+                    net.arrival(final.at[self.place(q, e, h)], self.slots + 2 * i + e, partner)
+
+        def forward(self):
+            for who, q, h, near, far, to in (
+                (same, xn, 0, 0, 4, to_y),
+                (jnp.logical_not(same), yn, 1, 3, 5, to_x),
+            ):
+                self.arrive(who, q, h, near)
+                for e in range(2):
+                    piece = final.at[self.place(q, e, h)]
+                    net.put(piece, piece, to, self.slots + 2 * far + e, who)
+
+        def gather(self):
+            self.arrive(same, xn, 1, 1)
+            other = jnp.logical_not(same)
+            self.arrive(other, yn, 0, 2)
+            self.arrive(other, dg, 0, 4)
+            self.arrive(other, dg, 1, 5)
+
+            @pl.when(same)
+            def _():
+                landed = final.at[self.place(s, 1 - c, 0, 2)]
+                net.arrival(landed, self.slots + 12 + 1 - c, partner)
+
+    spread_main, spread_early = Spread(0, side), Spread(rest, e_side)
+
     def keep_early():
         low, high = ahead.total()
-        own = pl.ds(al(s * share, share), share)
-        final[own, pl.ds(rest, e_side)] = low
-        final[own, pl.ds(rest + e_side, e_side)] = high
+        summed[:, pl.ds(rest, e_side)] = low
+        summed[:, pl.ds(rest + e_side, e_side)] = high
+        spread_early.send()
+
+    def pass_early():
+        spread_early.forward()
 
     def product(owner, start):
         w = weight[pl.ds(al(owner * rows, rows), rows), :]
@@ -857,9 +930,12 @@
         for i in range(1, nz):
             total = total + gain_dp[i]
         grad_gain[...] = total
+        written.append(net.load(grad_gain, out_gain))
 
     def send_terms():
         sums["mate"] = net.put(terms.at[1 - c], tap_mate, partner)
+        written.append(net.load(grad_value, out_value))
+        written.append(net.load(grad_gate, out_gate))
 
     def pair_sums():
         sums["mate"].wait_recv()
@@ -883,20 +959,14 @@
         for i in range(nz - 1):
             net.put(row_part, got_dp.at[z], at_chip(nearest(z, nz, i)), tap_slots + z)
 
-    def done(q, h):
-        return final.at[pl.ds(al(q * share, share), share), pl.ds(h * half // 2, half // 2)]
-
-    sent = {}
-
     def finish_rows():
         total = plane[nz - 1].astype(f32)
         for i in range(nz - 1):
             src = nearest(z, nz, i)
             net.arrival(got_z.at[src], z_slots + src, partner)
             total = total + got_z[src].astype(f32)
-        final[pl.ds(al(s * share, share), share), pl.ds(0, rest)] = total.astype(bf16)
-        for axis, h in (("x", 0), ("y", 1), ("y", 0), ("x", 1)):
-            sent[axis, h] = net.put(done(s, h), done(s, h), to_x if axis == "x" else to_y)
+        summed[:, pl.ds(0, rest)] = total.astype(bf16)
+        spread_main.send()
 
     def pair_terms():
         for i in range(nz - 1):
@@ -909,137 +979,151 @@
         sums["pair"] = net.put(both_parts, tap_other, partner)
 
     def spread_rows():
-        sent.pop(("x", 0)).wait_recv()
-        sent["low"] = net.put(done(xn, 0), done(xn, 0), to_y)
-        sent.pop(("y", 1)).wait_recv()
-        sent["high"] = net.put(done(yn, 1), done(yn, 1), to_x)
+        spread_main.forward()
 
     def keep_taps():
         sums["pair"].wait_recv()
         grad_taps[:, pl.ds(al(c * tap_width, tap_width), tap_width)] = both_parts[:tap_count]
         theirs = pl.ds(al((1 - c) * tap_width, tap_width), tap_width)
         grad_taps[:, theirs] = tap_other[:tap_count]
-
-    mine_rows = pl.ds(al(c * rows, rows), rows)
-    other_rows = pl.ds(al((1 - c) * rows, rows), rows)
+        written.append(net.load(grad_taps, out_taps))
 
     def gather_rows():
-        for copy in sent.values():
-            copy.wait_recv()
-        sums["last"] = net.put(final.at[other_rows], halves, partner)
-        grad_weight[:, mine] = final[mine_rows, :].astype(f32)
-
-    def keep():
-        sums["last"].wait_recv()
-        grad_weight[:, other] = halves[...].astype(f32)
+        spread_early.gather()
+        spread_main.gather()
 
     for step, *at in (
+        (conv_quarter, 0),
+        (tap_from, 0),
         (tap_from, 1),
-        (tap_from, 0),
-        (product_own,),
-        (conv_quarter, 0),
-        (tap_from, 2),
-        (conv_quarter, 3),
+        (conv_quarter, 2),
         (first, 0, 0),
         (first, 0, 1),
+        (tap_from, 2),
         (left_halo,),
         (first, 1, 0),
+        (conv_quarter, 3),
         (conv_quarter, 1),
-        (conv_quarter, 2),
         (first, 1, 1),
         (conv_head, 0),
+        (norm, 2),
         (first, 2, 0),
+        (norm, 3),
+        (second, 0, 0),
+        (norm, 1),
+        (second, 0, 1),
         (conv_head, 1),
-        (second, 0, 0),
-        (norm, 2),
+        (product_own,),
         (norm, 0),
-        (second, 0, 1),
-        (norm, 1),
-        (norm, 3),
         (first, 2, 1),
         (swap,),
+        (net.drain, 24),
+        (swap_done,),
         (second, 1, 0),
+        (net.drain, 24),
+        (multiply, 0),
         (second, 1, 1),
-        (swap_done,),
-        (multiply, 0),
-        (multiply, 1),
-        (product_mate,),
         (send_early, 0),
         (second, 2, 0),
+        (net.drain, 24),
+        (multiply, 3),
+        (third, 0, 0),
+        (net.drain, 24),
+        (multiply, 1),
+        (send_early, 3),
         (second, 2, 1),
-        (third, 0, 0),
+        (send_early, 1),
+        (net.drain, 24),
+        (multiply, 2),
         (third, 0, 1),
         (third, 1, 0),
+        (load, 0),
         (third, 1, 1),
-        (send_early, 1),
-        (load, 0),
+        (product_mate,),
+        (blocks_of, 1),
+        (blocks_of, 0),
         (load, 1),
-        (multiply, 2),
-        (blocks_of, 0),
+        (third, 2, 0),
+        (third, 2, 1),
+        (turn_y, 0),
+        (blocks_of, 2),
+        (send_early, 2),
         (turn_x, 0),
-        (turn_y, 0),
-        (blocks_of, 1),
-        (load, 2),
-        (third, 2, 0),
-        (multiply, 3),
-        (third, 2, 1),
-        (send_early, 2),
-        (blocks_of, 2),
-        (send_early, 3),
-        (turn_x, 1),
+        (net.drain, 24),
+        (back_head,),
+        (net.drain, 24),
+        (back, 0),
         (turn_y, 1),
-        (back_head,),
-        (back, 0),
+        (net.drain, 24),
         (back, 1),
         (back_tiles, 0),
+        (load, 2),
+        (back_tiles, 1),
+        (turn_x, 1),
+        (net.drain, 24),
+        (back_tiles, 2),
         (hand_on, 0),
-        (back_tiles, 1),
+        (back_tiles, 3),
+        (turn_y, 2),
+        (net.drain, 24),
+        (back_tiles, 4),
+        (add_early,),
+        (send_gain,),
+        (back_tiles, 5),
         (turn_x, 2),
-        (turn_y, 2),
-        (back_tiles, 2),
-        (send_gain,),
-        (add_early,),
-        (back_tiles, 3),
+        (load, 3),
         (hand_on, 1),
-        (back_tiles, 4),
-        (back_tiles, 5),
         (right_halo,),
-        (load, 3),
-        (back_tail, 0),
-        (hand_on, 2),
+        (net.drain, 24),
         (back_tiles, 6),
         (back_tiles, 7),
+        (back_tail, 0),
+        (pair_gain,),
+        (hand_on, 2),
+        (turn_early,),
         (turn_y, 3),
         (turn_x, 3),
         (back_tail, 1),
-        (turn_early,),
+        (net.drain, 24),
         (send_terms,),
         (pair_sums,),
-        (pair_gain,),
+        (keep_early,),
         (hand_on, 3),
-        (keep_early,),
         (finish_rows,),
+        (line_gain,),
         (add_terms,),
-        (line_gain,),
+        (net.drain, 10),
         (spread_rows,),
+        (keep_gain,),
+        (pass_early,),
         (pair_terms,),
+        (keep_taps,),
         (gather_rows,),
-        (keep_gain,),
-        (keep_taps,),
-        (keep,),
     ):
         step(*at)
-    net.finish()
+    net.drain()
+    for copy in written:
+        if isinstance(copy, tuple):
+            when(copy[1], copy[0].wait)
+        else:
+            copy.wait()
 
 
 def write_out(*refs):
-    held, outs, sems = refs[:5], refs[5:10], refs[10]
-    copies = [
-        pltpu.make_async_copy(a, b.at[0] if len(b.shape) > len(a.shape) else b, sems.at[i])
-        for i, (a, b) in enumerate(zip(held, outs))
-    ]
-    for copy in copies:
-        copy.start()
+    held, outs, wide, sems = refs[:5], refs[5:10], refs[10], refs[11]
+    copies = []
+
+    def start(src, dst):
+        copies.append(pltpu.make_async_copy(src, dst, sems.at[len(copies)]))
+        copies[-1].start()
+
+    for a, b in zip(held[:4], outs):
+        start(a, b.at[0] if len(b.shape) > len(a.shape) else b)
+    step = wide.shape[0] // 4
+    for i in range(4):
+        part = pl.ds(i * step, step)
+        wide[part, :] = held[4][part, :].astype(wide.dtype)
+        start(wide.at[part], outs[4].at[part])
     for copy in copies:
         copy.wait()
 
@@ -1064,7 +1148,7 @@
         return pltpu.VMEM(dims, dtype)
 
     hbm = pl.BlockSpec(memory_space=pltpu.MemorySpace.HBM)
-    remote = 60 + 30 * nz
+    remote = 31 + 28 * nz
     results = pl.pallas_call(
         fused,
         out_shape=[
@@ -1072,11 +1156,15 @@
             vmem(length, channels),
             vmem(tap_count, width, dtype=f32),
             vmem(1, channels, dtype=f32),
-            vmem(rows, channels, dtype=f32),
+            vmem(rows, channels),
         ],
         in_specs=[hbm] * 6,
-        out_specs=[VMEM] * 5,
+        out_specs=[pl.BlockSpec(memory_space=pl.ANY)] * 5,
         scratch_shapes=[
+            vmem(length, channels),
+            vmem(length, channels),
+            vmem(tap_count, width, dtype=f32),
+            vmem(1, channels, dtype=f32),
             vmem(length, channels),
             vmem(length, channels),
             vmem(2 * length, channels),
@@ -1097,8 +1185,7 @@
             vmem(nz, share, side),
             vmem(nz, share, half - lead),
             vmem(nz, share, half - lead),
-            vmem(2 * rows, half),
-            vmem(rows, half),
+            vmem(share, half),
             vmem(nz, share, side),
             vmem(nz, share, side),
             vmem(nz, 2 * rows, lead),
@@ -1129,9 +1216,9 @@
             vmem(nsp, 1, channels, dtype=f32),
             vmem(1, channels, dtype=f32),
             vmem(nz, 1, channels, dtype=f32),
+            pltpu.SemaphoreType.DMA((48,)),
             pltpu.SemaphoreType.DMA((remote,)),
-            pltpu.SemaphoreType.DMA((remote,)),
-            pltpu.SemaphoreType.DMA((8,)),
+            pltpu.SemaphoreType.DMA((12,)),
         ],
         compiler_params=pltpu.CompilerParams(
             collective_id=7, has_side_effects=True, vmem_limit_bytes=58 * 1024 * 1024
@@ -1146,9 +1233,9 @@
             shape(1, channels, dtype=f32),
             shape(rows, channels, dtype=f32),
         ],
-        in_specs=[VMEM] * 5,
+        in_specs=[pl.BlockSpec(memory_space=pl.ANY)] * 4 + [VMEM],
         out_specs=[hbm] * 5,
-        scratch_shapes=[pltpu.SemaphoreType.DMA((5,))],
+        scratch_shapes=[vmem(rows, channels, dtype=f32), pltpu.SemaphoreType.DMA((8,))],
         compiler_params=pltpu.CompilerParams(vmem_limit_bytes=8 * 1024 * 1024),
     )(*results)
     return (grad_value, grad_gate, grad_taps, grad_gain[0], grad_weight)

time: 87.9 us -> 82.8 us (0.942)
  Pallas kernels: 87.1 us -> 82 us
    pallas_call x1, Pallas kernels: 85 us -> 79.9 us  [fused_body(): pl.pallas_call(fused, out_shape=[vmem(length, channels), vmem(length, cha...]
where the time goes in v4:
time: 82.8 us; the launch traced here: 82.6 us
  Pallas kernels  82 us (99%)
    pallas_call x1, Pallas kernels, fused_body(): pl.pallas_call(fused, out_shape=[vmem(length, channels), vmem(length, cha...  79.9 us
    pallas_call x1, Pallas kernels, fused_body(): pl.pallas_call(write_out, out_shape=[shape(1, length, channels), shape(1,...  2.1 us

profile of v4, /device:TPU:1, one launch (start us, length us, event | category | flops | bytes accessed | tf_op | source)
XLA Modules:
  0.0 82.6 jit_solution(17884171037814578660)
XLA Ops:
  0.6 79.9 %shard_map.101 = (bf16[256,2048]{1,0:T(8,128)(2,1)S(1)}, bf16[256,2048]{1,0:T(8,128)(2,1)S(1)}, f32[31,512]{1,0:T(8,128)S(1)}, f32[1,2048]{1,0:T(1,128)S(1)}, bf16[256,2048]{1,0:T(8,128)(2,1)S(1)}) custom-call(bf16[1,256,2048]{2,1,0:T(8,128)(2,1)} %value_hbm.1, bf16[1,256,2048]{2,1,0:T(8,128)(2,1)} %gate_hbm.1, bf16[1,256,2048]{2,1,0:T(8,128)(2,1)} %up_hbm.1, ...), custom_call_target="tpu_custom_call" | custom-call | tf_op jit(solution)/shard_map/pallas_call | solution.py:1152
  80.5 2.1 %shard_map.102 = (bf16[1,256,2048]{2,1,0:T(8,128)(2,1)}, bf16[1,256,2048]{2,1,0:T(8,128)(2,1)}, f32[31,512]{1,0:T(8,128)}, f32[1,2048]{1,0:T(1,128)}, f32[256,2048]{1,0:T(8,128)}) custom-call(bf16[256,2048]{1,0:T(8,128)(2,1)S(1)} %get-tuple-element.15.refs_0_, bf16[256,2048]{1,0:T(8,128)(2,1)S(1)} %get-tuple-element.16.refs_1_, ...), custom_call_target="tpu_custom_call" | custom-call | tf_op jit(solution)/shard_map/pallas_call | solution.py:1227

commit v5 on v4

--- a/solution.py
+++ b/solution.py
@@ -994,9 +994,9 @@
 
     for step, *at in (
         (conv_quarter, 0),
-        (tap_from, 0),
         (tap_from, 1),
         (conv_quarter, 2),
+        (tap_from, 0),
         (first, 0, 0),
         (first, 0, 1),
         (tap_from, 2),
@@ -1007,10 +1007,10 @@
         (first, 1, 1),
         (conv_head, 0),
         (norm, 2),
+        (norm, 1),
         (first, 2, 0),
         (norm, 3),
         (second, 0, 0),
-        (norm, 1),
         (second, 0, 1),
         (conv_head, 1),
         (product_own,),
@@ -1021,15 +1021,15 @@
         (swap_done,),
         (second, 1, 0),
         (net.drain, 24),
+        (multiply, 1),
+        (net.drain, 24),
         (multiply, 0),
+        (send_early, 0),
         (second, 1, 1),
-        (send_early, 0),
         (second, 2, 0),
         (net.drain, 24),
         (multiply, 3),
         (third, 0, 0),
-        (net.drain, 24),
-        (multiply, 1),
         (send_early, 3),
         (second, 2, 1),
         (send_early, 1),

time: 82.8 us -> 82.4 us (level)
  no operation moved by 1% of the time
where the time goes in v5:
time: 82.4 us; the launch traced here: 82.3 us
  Pallas kernels  81.6 us (99%)
    pallas_call x1, Pallas kernels, fused_body(): pl.pallas_call(fused, out_shape=[vmem(length, channels), vmem(length, cha...  79.5 us
    pallas_call x1, Pallas kernels, fused_body(): pl.pallas_call(write_out, out_shape=[shape(1, length, channels), shape(1,...  2.1 us

profile of v5, /device:TPU:1, one launch (start us, length us, event | category | flops | bytes accessed | tf_op | source)
XLA Modules:
  0.0 82.3 jit_solution(1830833599970151718)
XLA Ops:
  0.6 79.5 %shard_map.101 = (bf16[256,2048]{1,0:T(8,128)(2,1)S(1)}, bf16[256,2048]{1,0:T(8,128)(2,1)S(1)}, f32[31,512]{1,0:T(8,128)S(1)}, f32[1,2048]{1,0:T(1,128)S(1)}, bf16[256,2048]{1,0:T(8,128)(2,1)S(1)}) custom-call(bf16[1,256,2048]{2,1,0:T(8,128)(2,1)} %value_hbm.1, bf16[1,256,2048]{2,1,0:T(8,128)(2,1)} %gate_hbm.1, bf16[1,256,2048]{2,1,0:T(8,128)(2,1)} %up_hbm.1, ...), custom_call_target="tpu_custom_call" | custom-call | tf_op jit(solution)/shard_map/pallas_call | solution.py:1152
  80.2 2.1 %shard_map.102 = (bf16[1,256,2048]{2,1,0:T(8,128)(2,1)}, bf16[1,256,2048]{2,1,0:T(8,128)(2,1)}, f32[31,512]{1,0:T(8,128)}, f32[1,2048]{1,0:T(1,128)}, f32[256,2048]{1,0:T(8,128)}) custom-call(bf16[256,2048]{1,0:T(8,128)(2,1)S(1)} %get-tuple-element.15.refs_0_, bf16[256,2048]{1,0:T(8,128)(2,1)S(1)} %get-tuple-element.16.refs_1_, ...), custom_call_target="tpu_custom_call" | custom-call | tf_op jit(solution)/shard_map/pallas_call | solution.py:1227
